TPU v7x, 32 devices: a whole 2x2x4 slice. The times are simulated.
32 devices in a mesh: sp: 8 (over z, x), tp: 4 (over y, core).
Axes of the slice: x: 2, y: 2, z: 4, core: 2. Of those that a mesh axis runs over, the one named last changes fastest.
Arguments:
- tokens: bfloat16 [4096, 2048], P(('sp', 'tp')), may hold values from -6 to 6
- input_norm_scale: bfloat16 [2048], replicated, may hold values from 0.099609375 to 1.8984375
- outer_gate_weight: bfloat16 [2048, 1024], P('sp', 'tp'), may hold values from -0.125 to 0.125
- inner_gate_weight: bfloat16 [2048, 1024], P('sp', 'tp'), may hold values from -0.125 to 0.125
- value_weight_matrix: bfloat16 [2048, 1024], P('sp', 'tp'), may hold values from -0.125 to 0.125
- output_gate_weight: bfloat16 [2048, 1024], P('sp', 'tp'), may hold values from -0.125 to 0.125
- state_input_weight: bfloat16 [2048, 1024], P('sp', 'tp'), may hold values from -0.125 to 0.125
- write_key_weight: bfloat16 [2048, 512], P('sp', 'tp'), may hold values from -0.125 to 0.125
- read_key_weight: bfloat16 [2048, 512], P('sp', 'tp'), may hold values from -0.125 to 0.125
- step_size_weight: bfloat16 [2048, 16], P(None, 'tp'), may hold values from -0.125 to 0.125
- gated_conv_weight: bfloat16 [3, 1024], P(None, 'tp'), may hold values from -3.5 to 3.5
- input_conv_weight: bfloat16 [4, 1024], P(None, 'tp'), may hold values from -3 to 3
- write_conv_weight: bfloat16 [4, 512], P(None, 'tp'), may hold values from -3 to 3
- read_conv_weight: bfloat16 [4, 512], P(None, 'tp'), may hold values from -3 to 3
- step_size_bias: float32 [16], P('tp'), may hold values from -1 to 0.5
- log_decay_rate: float32 [16], P('tp'), may hold values from -16 to -2.5, as said below
- decay_spikes: float32 [16, 4096], P('tp', 'sp'), may hold values from -1 to 0, as said below
- direct_path_weight: float32 [16], P('tp'), may hold values from 0.5 to 2
- head_norm_scale: bfloat16 [1024], P('tp'), may hold values from 0.099609375 to 1.8984375
- conv_output_weight: bfloat16 [1024, 2048], P('tp', 'sp'), may hold values from -0.125 to 0.125
- state_output_weight: bfloat16 [1024, 2048], P('tp', 'sp'), may hold values from -0.125 to 0.125
Outputs:
- mixed: bfloat16 [4096, 2048], P(('sp', 'tp'))
Inputs may be any that keep to these rules, and one draw needn't show every extreme that they name: `log_decay_rate`: one value a head. `decay_spikes`: never positive.
All inputs are finite; a program needn't handle non-finite values.
Results may differ from a plain program's by a relative error of at most 0.017.
Values may be sent and summed in bfloat16 or wider, within the bound.
A program may use at most 128 MiB of HBM per device.

v0:
```python
import jax
import jax.numpy as jnp
from jax import lax
from jax.sharding import PartitionSpec as P

HEAD_DIM = 64
STATE = 128
BLOCK = 64


epsilon = 1e-05
highest = lax.Precision.HIGHEST


def shifted(shard, axis, by):
    devices = lax.axis_size(axis)
    pairs = [(i, i + by) for i in range(devices) if 0 <= i + by < devices]
    return lax.ppermute(shard, axis, pairs)


def prefix(shard, axis, combine, identity):
    devices, index = (lax.axis_size(axis), lax.axis_index(axis))
    everything = jax.tree.map(
        lambda part, kind: lax.all_gather(part.astype(kind), axis),
        shard,
        (jnp.bfloat16, jnp.bfloat16),
    )
    start = jax.tree.map(
        lambda part, zero: jnp.broadcast_to(jnp.asarray(zero, part.dtype), part.shape),
        shard,
        identity,
    )

    def turn(k, before):
        reached = k < index
        new = combine(
            before, jax.tree.map(lambda part, own: part[k].astype(own.dtype), everything, shard)
        )
        return jax.tree.map(lambda a, b: jnp.where(reached, a, b), new, before)

    return lax.fori_loop(0, devices, turn, start)


def causal_taps(values, rim_rows, tap_weights):
    tap_count = tap_weights.shape[0]
    length = values.shape[0]
    padded = jnp.concatenate([rim_rows, values], axis=0)
    running = tap_weights[0] * padded[0:length]
    for offset in range(1, tap_count):
        running = running + tap_weights[offset] * padded[offset : offset + length]
    return running


def combine_states(earlier, later):
    return (earlier[0] * later[0], earlier[1] * later[0][:, None, None] + later[1])


def per_device(
    tokens,
    input_norm_scale,
    outer_gate_weight,
    inner_gate_weight,
    value_weight_matrix,
    output_gate_weight,
    state_input_weight,
    write_key_weight,
    read_key_weight,
    step_size_weight,
    gated_conv_weight,
    input_conv_weight,
    write_conv_weight,
    read_conv_weight,
    step_size_bias,
    log_decay_rate,
    decay_spikes,
    direct_path_weight,
    head_norm_scale,
    conv_output_weight,
    state_output_weight,
):
    token_rows = tokens.astype(jnp.float32)
    scaled = token_rows * lax.rsqrt(
        jnp.mean(token_rows * token_rows, axis=1, keepdims=True) + epsilon
    )
    normed_own = (scaled * input_norm_scale.astype(jnp.float32)).astype(jnp.bfloat16)
    normed = lax.all_gather(normed_own, "tp", axis=0, tiled=True)
    length = normed.shape[0]
    pieces = (
        lax.all_gather(outer_gate_weight, "sp", axis=0, tiled=True),
        lax.all_gather(inner_gate_weight, "sp", axis=0, tiled=True),
        lax.all_gather(value_weight_matrix, "sp", axis=0, tiled=True),
        lax.all_gather(output_gate_weight, "sp", axis=0, tiled=True),
        lax.all_gather(state_input_weight, "sp", axis=0, tiled=True),
        lax.all_gather(write_key_weight, "sp", axis=0, tiled=True),
        lax.all_gather(read_key_weight, "sp", axis=0, tiled=True),
    )
    projected = tuple(
        (jnp.dot(normed, weight_rows, preferred_element_type=jnp.float32) for weight_rows in pieces)
    )
    outer_gate, inner_gate, conv_input, out_gate, state_input, write_keys, read_keys = [
        member.astype(jnp.bfloat16) for member in projected
    ]
    step_raw = jnp.dot(normed, step_size_weight, preferred_element_type=jnp.float32)
    short_rim = gated_conv_weight.shape[0] - 1
    state_rim = input_conv_weight.shape[0] - 1
    rim_rows = shifted(
        (
            inner_gate[length - short_rim :],
            conv_input[length - short_rim :],
            state_input[length - state_rim :],
            write_keys[length - state_rim :],
            read_keys[length - state_rim :],
        ),
        "sp",
        1,
    )
    product = inner_gate.astype(jnp.float32) * conv_input.astype(jnp.float32)
    rim_product = rim_rows[0].astype(jnp.float32) * rim_rows[1].astype(jnp.float32)
    mixer_part = (
        outer_gate.astype(jnp.float32)
        * causal_taps(product, rim_product, gated_conv_weight.astype(jnp.float32))
    ).astype(jnp.bfloat16)
    seq_input = jax.nn.silu(
        causal_taps(
            state_input.astype(jnp.float32),
            rim_rows[2].astype(jnp.float32),
            input_conv_weight.astype(jnp.float32),
        )
    )
    seq_write = jax.nn.silu(
        causal_taps(
            write_keys.astype(jnp.float32),
            rim_rows[3].astype(jnp.float32),
            write_conv_weight.astype(jnp.float32),
        )
    )
    seq_read = jax.nn.silu(
        causal_taps(
            read_keys.astype(jnp.float32),
            rim_rows[4].astype(jnp.float32),
            read_conv_weight.astype(jnp.float32),
        )
    )
    discrete_step = jax.nn.softplus(step_raw + step_size_bias[None, :])
    step_logarithm = discrete_step * (-jnp.exp(log_decay_rate))[None, :] + decay_spikes.T
    heads_here = discrete_step.shape[1]
    groups_here = seq_write.shape[1] // STATE
    per_group = heads_here // groups_here
    blocks = length // BLOCK
    input_blocks = seq_input.reshape(blocks, BLOCK, heads_here, HEAD_DIM)
    weighted = input_blocks * discrete_step.reshape(blocks, BLOCK, heads_here, 1)
    write_blocks = jnp.repeat(
        seq_write.reshape(blocks, BLOCK, groups_here, STATE), per_group, axis=2
    )
    read_blocks = jnp.repeat(seq_read.reshape(blocks, BLOCK, groups_here, STATE), per_group, axis=2)
    cumulative = jnp.cumsum(step_logarithm.reshape(blocks, BLOCK, heads_here), axis=1)
    causal = lax.broadcasted_iota(jnp.int32, (BLOCK, BLOCK), 0) >= lax.broadcasted_iota(
        jnp.int32, (BLOCK, BLOCK), 1
    )
    scores = jnp.einsum("clhm,cshm->clsh", read_blocks, write_blocks, precision=highest)
    damping = jnp.exp(
        jnp.where(
            causal[None, :, :, None],
            cumulative[:, :, None, :] - cumulative[:, None, :, :],
            -jnp.inf,
        )
    )
    within_block = jnp.einsum("clsh,cshp->clhp", scores * damping, weighted, precision=highest)
    to_end = jnp.exp(cumulative[:, -1:, :] - cumulative)
    block_states = jnp.einsum(
        "cshm,cshp->chpm", write_blocks * to_end[..., None], weighted, precision=highest
    )
    block_logs = cumulative[:, -1, :]

    def advance(carried_state, inputs):
        contribution, block_log = inputs
        return (carried_state * jnp.exp(block_log)[:, None, None] + contribution, carried_state)

    own_total, own_before = lax.scan(
        advance, jnp.zeros(block_states.shape[1:], jnp.float32), (block_states, block_logs)
    )
    total_log = jnp.sum(block_logs, axis=0)
    arriving = prefix(
        (jnp.exp(total_log), own_total),
        "sp",
        combine_states,
        (jnp.ones_like(total_log), jnp.zeros_like(own_total)),
    )[1]
    before_logs = jnp.cumsum(block_logs, axis=0) - block_logs
    entering = own_before + jnp.exp(before_logs)[:, :, None, None] * arriving[None]
    from_before = (
        jnp.einsum("clhm,chpm->clhp", read_blocks, entering, precision=highest)
        * jnp.exp(cumulative)[..., None]
    )
    head_out = within_block + from_before + direct_path_weight[None, None, :, None] * input_blocks
    head_out = head_out.reshape(length, heads_here * HEAD_DIM)
    gated_heads = (head_out * jax.nn.silu(out_gate.astype(jnp.float32))).reshape(
        length, heads_here, HEAD_DIM
    )
    normalized = gated_heads * lax.rsqrt(
        jnp.mean(gated_heads * gated_heads, axis=2, keepdims=True) + epsilon
    )
    state_part = (
        normalized.reshape(length, heads_here * HEAD_DIM) * head_norm_scale.astype(jnp.float32)
    ).astype(jnp.bfloat16)
    wide_mixer, wide_state = (
        lax.all_gather(conv_output_weight, "sp", axis=1, tiled=True),
        lax.all_gather(state_output_weight, "sp", axis=1, tiled=True),
    )
    return lax.psum_scatter(
        (
            jnp.dot(mixer_part, wide_mixer, preferred_element_type=jnp.float32)
            + jnp.dot(state_part, wide_state, preferred_element_type=jnp.float32)
        ).astype(jnp.bfloat16),
        "tp",
        scatter_dimension=0,
        tiled=True,
    )


def solution(mesh):
    placed = (
        P(("sp", "tp"), None),
        P(),
        P("sp", "tp"),
        P("sp", "tp"),
        P("sp", "tp"),
        P("sp", "tp"),
        P("sp", "tp"),
        P("sp", "tp"),
        P("sp", "tp"),
        P(None, "tp"),
        P(None, "tp"),
        P(None, "tp"),
        P(None, "tp"),
        P(None, "tp"),
        P("tp"),
        P("tp"),
        P("tp", "sp"),
        P("tp"),
        P("tp"),
        P("tp", "sp"),
        P("tp", "sp"),
    )
    return jax.shard_map(
        per_device, mesh=mesh, in_specs=placed, out_specs=P(("sp", "tp"), None), check_vma=False
    )
```

profile of v0, /device:TPU:0, one launch (start us, length us, event | category | flops | bytes accessed | tf_op | source)
XLA Modules:
  0.0 369.9 jit_solution(7055636501463184764)
XLA Ops:
  8.7 2.0 fusion.14
  15.6 35.2 %all_gather.46 = bf16[2048,128]{1,0:T(8,128)(2,1)} all-gather(bf16[256,128]{1,0:T(8,128)(2,1)S(1)} %copy-done.7), channel_id=1, replica_groups=mesh['sp'=8,'tp'=4] {'sp'}, dimensions={0}, use_global_device_ids=true | all-gather | bytes 589824 | tf_op jit(solution)/shard_map/all_gather | solution.py:94
  51.4 33.7 %all_gather.47 = bf16[2048,128]{1,0:T(8,128)(2,1)} all-gather(bf16[256,128]{1,0:T(8,128)(2,1)S(1)} %copy-done.8), channel_id=1, replica_groups=mesh['sp'=8,'tp'=4] {'sp'}, dimensions={0}, use_global_device_ids=true | all-gather | bytes 589824 | tf_op jit(solution)/shard_map/all_gather | solution.py:95
  87.5 2.4 bitcast_add_fusion.1
  90.2 6.3 %fusion.75 = f32[8,64,4]{2,0,1:T(8,128)S(1)} fusion(f32[8,64,4]{2,0,1:T(8,128)S(1)} %copy.54), kind=kOutput, calls=%fused_computation.130 | output fusion | flops 129024 | bytes 16384 | tf_op jit(solution)/shard_map/jit(cumsum)/reduce_window_sum | solution.py:156
  96.7 1.9 fusion.73
  98.7 4.0 %collective-permute-start.2 = (bf16[3,256]{1,0:T(4,128)(2,1)S(1)}, bf16[3,256]{1,0:T(4,128)(2,1)S(1)}, u32[]{:S(2)}, u32[]{:S(2)}) collective-permute-start(bf16[3,256]{1,0:T(4,128)(2,1)S(1)} %slice.137), channel_id=1, source_target_pairs={{0,4},{4,8},{8,12},{12,16},{16,20},{20,24},{24,28},{1,5},{5,9},{9,... | collective-permute-start | bytes 4616 | tf_op jit(solution)/shard_map/ppermute | solution.py:18
  102.7 1.7 fusion.72
  105.0 2.5 collective-permute-start.3
  108.7 13.8 %all-gather.15.cloned.1.call-done = bf16[2048,256]{1,0:T(8,128)(2,1)} async-done(((bf16[256,256]{1,0:T(8,128)(2,1)}), bf16[2048,256]{1,0:T(8,128)(2,1)}) %all-gather.15.cloned.1.call-update) | async-done | bytes 1048592 | tf_op jit(solution)/shard_map/all_gather | solution.py:90
  122.6 1.9 convolution_convert_fusion.3
  125.3 2.5 fusion.71
  127.9 35.7 %all-gather.17.cloned.1.call-done = bf16[2048,256]{1,0:T(8,128)(2,1)} async-done(((bf16[256,256]{1,0:T(8,128)(2,1)}), bf16[2048,256]{1,0:T(8,128)(2,1)}) %all-gather.17.cloned.1.call-update) | async-done | bytes 1048592 | tf_op jit(solution)/shard_map/all_gather | solution.py:91
  163.6 2.9 convert_multiply_fusion.2
  167.5 19.2 %all-reduce = bf16[32]{0:T(256)(128)(2,1)S(1)} all-reduce(bf16[32]{0:T(256)(128)(2,1)S(1)} %dynamic-update-slice), channel_id=2, replica_groups=mesh['sp'=8,'tp'=4] {'sp'}, use_global_device_ids=true, to_apply=%add | all-reduce | flops 32 | bytes 128
  188.1 2.5 collective-permute-start.4
  193.0 2.2 collective-permute-start
  198.9 2.7 fusion.5
  201.6 3.0 all-gather.13.cloned.1.call-done
  204.6 40.0 %all-gather.19.cloned.1.call-done = bf16[256,2048]{1,0:T(8,128)(2,1)} async-done(((bf16[256,256]{1,0:T(8,128)(2,1)}), bf16[256,2048]{1,0:T(8,128)(2,1)}) %all-gather.19.cloned.1.call-update) | async-done | bytes 1048592 | tf_op jit(solution)/shard_map/all_gather | solution.py:207
  244.6 6.3 %fusion.11 = f32[512,2048]{1,0:T(8,128)} fusion(bf16[256,2048]{1,0:T(8,128)(2,1)} %all-gather.19.cloned.1.call-done, bf16[512,2048]{1,0:T(8,128)(2,1)S(1)} %copy-done.1, bf16[2048,256]{1,0:T(8,128)(2,1)} %all-gather.13.cloned.1.call-done, f32[2,256]{1,0:T(2,128)S(1)} %convert_multiply_fusion.3, f32[512,256]{1,0:T(8,128)} %get-tuple-element.220, ...), kind=kOutput, calls=%fused_computation.27 | convolution fusion | flops 1075183616 | bytes 8918016 | tf_op jit(solution)/shard_map/dot_general | solution.py:212
  252.0 2.5 reshape.111
  256.1 3.2 fusion.17
  259.4 13.5 %while.27 = (s32[]{:T(128)}, f32[4,64,128]{2,1,0:T(8,128)S(1)}, f32[8,4,64,128]{3,2,1,0:T(8,128)}, f32[8,4]{1,0:T(8,128)S(1)}, f32[8,4,64,128]{3,2,1,0:T(8,128)}, /*index=5*/s32[]{:T(128)}, s32[]{:T(128)}) while((s32[]{:T(128)}, f32[4,64,128]{2,1,0:T(8,128)S(1)}, f32[8,4,64,128]{3,2,1,0:T(8,128)}, f32[8,4]{1,0:T(8,128)S(1)}, ...), condition=%wide.region_3.4_spmd.clone, body=%wide.region_2.3_spmd.clone.sunk | while | flops 131075 | bytes 656016 | solution.py:179
  272.9 33.8 %all-gather.1 = bf16[32,64,128]{2,1,0:T(8,128)(2,1)} all-gather(bf16[4,64,128]{2,1,0:T(8,128)(2,1)S(1)} %convert_element_type.157), channel_id=3, replica_groups=mesh['sp'=8,'tp'=4] {'sp'}, dimensions={0}, use_global_device_ids=true | all-gather | bytes 589824 | tf_op jit(solution)/shard_map/all_gather | solution.py:24
  306.6 7.7 %while.28 = (s32[]{:T(128)}, f32[4,64,128]{2,1,0:T(8,128)S(1)}, s32[]{:T(128)}, bf16[8,4]{1,0:T(8,128)(2,1)S(1)}, bf16[8,4,64,128]{3,2,1,0:T(8,128)(2,1)}, /*index=5*/s32[]{:T(128)}, s32[]{:T(128)}) while((s32[]{:T(128)}, f32[4,64,128]{2,1,0:T(8,128)S(1)}, s32[]{:T(128)}, bf16[8,4]{1,0:T(8,128)(2,1)S(1)}, ...), condition=%wide.region_7.8_spmd.clone, body=%wide.region_6.7_spmd.clone.sunk | while | flops 163848 | bytes 327825 | solution.py:41
  314.4 2.5 convolution_bitcast_fusion.1
  316.9 2.9 fusion.6
  322.9 2.1 fusion.74
  325.5 2.9 all-gather.25.cloned.1.call-done
  328.4 4.6 %add_convert_fusion = bf16[512,2048]{1,0:T(8,128)(2,1)} fusion(f32[512,2048]{1,0:T(8,128)} %fusion.11, bf16[256,2048]{1,0:T(8,128)(2,1)} %all-gather.25.cloned.1.call-done, f32[512,256]{1,0:T(8,128)S(1)} %get-tuple-element.231, f32[512,256]{1,0:T(8,128)S(1)} %copy.68, f32[256]{0:T(256)S(1)} %copy-done.12), kind=kOutput, calls=%fused_computation.8 | convolution fusion | flops 539361280 | bytes 8389632 | tf_op jit(solution)/shard_map/dot_general | solution.py:213
  333.1 30.3 %reduce-scatter.2.cloned.1.call-done = bf16[128,2048]{1,0:T(8,128)(2,1)} async-done(((bf16[512,2048]{1,0:T(8,128)(2,1)}), bf16[128,2048]{1,0:T(8,128)(2,1)}) %reduce-scatter.2.cloned.1.call-update) | async-done | bytes 524304 | tf_op jit(solution)/shard_map/reduce_scatter | solution.py:210
  (164 shorter events, 47.8 us)
Async XLA Ops:
  6.5 80.9 %copy-start = (bf16[2048,4]{0,1:T(4,128)(2,1)S(1)}, bf16[2048,4]{0,1:T(4,128)(2,1)}, u32[]{:S(2)}) copy-start(bf16[2048,4]{0,1:T(4,128)(2,1)} %param.34) | copy-start | bytes 49156
  6.5 9.0 %copy-start.10 = (bf16[4,256]{1,0:T(4,128)(2,1)S(1)}, bf16[4,256]{1,0:T(4,128)(2,1)}, u32[]{:S(2)}) copy-start(bf16[4,256]{1,0:T(4,128)(2,1)} %param.36) | copy-start | bytes 6148
  6.5 9.0 %copy-start.7 = (bf16[256,128]{1,0:T(8,128)(2,1)S(1)}, bf16[256,128]{1,0:T(8,128)(2,1)}, u32[]{:S(2)}) copy-start(bf16[256,128]{1,0:T(8,128)(2,1)} %param.32) | copy-start | bytes 196612
  6.5 44.3 %copy-start.13 = (bf16[4,128]{1,0:T(4,128)(2,1)S(1)}, bf16[4,128]{1,0:T(4,128)(2,1)}, u32[]{:S(2)}) copy-start(bf16[4,128]{1,0:T(4,128)(2,1)} %param.37) | copy-start | bytes 3076
  6.5 44.8 %copy-start.18 = (f32[4]{0:T(128)S(1)}, f32[4]{0:T(128)}, u32[]{:S(2)}) copy-start(f32[4]{0:T(128)} %param.40) | copy-start | bytes 52
  6.5 44.8 %copy-start.8 = (bf16[256,128]{1,0:T(8,128)(2,1)S(1)}, bf16[256,128]{1,0:T(8,128)(2,1)}, u32[]{:S(2)}) copy-start(bf16[256,128]{1,0:T(8,128)(2,1)} %param.33) | copy-start | bytes 196612
  6.6 80.9 %all-gather.11.cloned.1.call-start = ((), (), s32[]{:S(2)}) async-start(), calls=%async_computation.1 | async-start | bytes 2621440 | tf_op jit(solution)/shard_map/all_gather | solution.py:86
  7.3 77.7 %copy-start.14 = (bf16[4,128]{1,0:T(4,128)(2,1)S(1)}, bf16[4,128]{1,0:T(4,128)(2,1)}, u32[]{:S(2)}) copy-start(bf16[4,128]{1,0:T(4,128)(2,1)} %param.38) | copy-start | bytes 3076
  7.3 78.3 %copy-start.11 = (bf16[3,256]{1,0:T(4,128)(2,1)S(1)}, bf16[3,256]{1,0:T(4,128)(2,1)}, u32[]{:S(2)}) copy-start(bf16[3,256]{1,0:T(4,128)(2,1)} %param.35) | copy-start | bytes 4612
  7.4 78.3 %copy-start.19 = (bf16[256]{0:T(256)(128)(2,1)S(1)}, bf16[256]{0:T(256)(128)(2,1)}, u32[]{:S(2)}) copy-start(bf16[256]{0:T(256)(128)(2,1)} %param.43) | copy-start | bytes 1540
  7.4 78.9 %copy-start.20 = (u32[32]{0:T(128)S(1)}, u32[32]{0:T(128)}, u32[]{:S(2)}) copy-start(u32[32]{0:T(128)} %constant.73) | copy-start | bytes 388
  7.4 80.1 %copy-start.9 = (f32[4,512]{1,0:T(4,128)S(1)}, f32[4,512]{1,0:T(4,128)}, u32[]{:S(2)}) copy-start(f32[4,512]{1,0:T(4,128)} %param.41) | copy-start | bytes 24580
  7.4 80.1 %copy-start.16 = (f32[4]{0:T(128)S(1)}, f32[4]{0:T(128)}, u32[]{:S(2)}) copy-start(f32[4]{0:T(128)} %param.39) | copy-start | bytes 52
  10.7 86.0 %all-gather.21.cloned.1.call-start = ((), (), s32[]{:S(2)}) async-start(), calls=%async_computation.6 | async-start | bytes 1179648 | tf_op jit(solution)/shard_map/all_gather | solution.py:93
  11.5 111.1 %all-gather.15.cloned.1.call-start = ((), (), s32[]{:S(2)}) async-start(), calls=%async_computation.3 | async-start | bytes 1179648 | tf_op jit(solution)/shard_map/all_gather | solution.py:90
  12.2 151.3 %all-gather.17.cloned.1.call-start = ((), (), s32[]{:S(2)}) async-start(), calls=%async_computation.4 | async-start | bytes 1179648 | tf_op jit(solution)/shard_map/all_gather | solution.py:91
  12.8 191.8 %all-gather.13.cloned.1.call-start = ((), (), s32[]{:S(2)}) async-start(), calls=%async_computation.2 | async-start | bytes 1179648 | tf_op jit(solution)/shard_map/all_gather | solution.py:89
  13.4 231.3 %all-gather.19.cloned.1.call-start = ((), (), s32[]{:S(2)}) async-start(), calls=%async_computation.5 | async-start | bytes 1179648 | tf_op jit(solution)/shard_map/all_gather | solution.py:207
  14.0 308.9 %all-gather.23.cloned.1.call-start = ((), (), s32[]{:S(2)}) async-start(), calls=%async_computation.7 | async-start | bytes 1179648 | tf_op jit(solution)/shard_map/all_gather | solution.py:92
  14.7 313.7 %all-gather.25.cloned.1.call-start = ((), (), s32[]{:S(2)}) async-start(), calls=%async_computation.8 | async-start | bytes 1179648 | tf_op jit(solution)/shard_map/all_gather | solution.py:208
  15.5 347.9 %reduce-scatter.2.cloned.1.call-start = ((), (), s32[]{:S(2)}) async-start(), calls=%async_computation.9 | async-start | bytes 2621440 | tf_op jit(solution)/shard_map/reduce_scatter | solution.py:210
  87.5 9.2 %copy-start.1 = (bf16[512,2048]{1,0:T(8,128)(2,1)S(1)}, bf16[512,2048]{1,0:T(8,128)(2,1)}, u32[]{:S(2)}) copy-start(bf16[512,2048]{1,0:T(8,128)(2,1)} %all-gather.11.cloned.1.call-done) | copy-start | bytes 6291460
  98.7 152.2 %collective-permute-start.2 = (bf16[3,256]{1,0:T(4,128)(2,1)S(1)}, bf16[3,256]{1,0:T(4,128)(2,1)S(1)}, u32[]{:S(2)}, u32[]{:S(2)}) collective-permute-start(bf16[3,256]{1,0:T(4,128)(2,1)S(1)} %slice.137), channel_id=1, source_target_pairs={{0,4},{4,8},{8,12},{12,16},{16,20},{20,24},{24,28},{1,5},{5,9},{9,... | collective-permute-start | bytes 4616 | tf_op jit(solution)/shard_map/ppermute | solution.py:18
  105.0 90.2 %collective-permute-start.3 = (bf16[3,128]{1,0:T(4,128)(2,1)}, bf16[3,128]{1,0:T(4,128)(2,1)}, u32[]{:S(2)}, u32[]{:S(2)}) collective-permute-start(bf16[3,128]{1,0:T(4,128)(2,1)} %slice.145), channel_id=1, source_target_pairs={{0,4},{4,8},{8,12},{12,16},{16,20},{20,24},{24,28},{1,5},{5,9},{9,... | collective-permute-start | bytes 2312 | tf_op jit(solution)/shard_map/ppermute | solution.py:18
  127.9 62.7 %copy-start.5 = (f32[8,64,4]{2,0,1:T(8,128)S(1)}, f32[8,64,4]{2,0,1:T(8,128)}, u32[]{:S(2)}) copy-start(f32[8,64,4]{2,0,1:T(8,128)} %get-tuple-element.203) | copy-start | bytes 24580
  188.1 8.6 %collective-permute-start.4 = (bf16[3,128]{1,0:T(4,128)(2,1)}, bf16[3,128]{1,0:T(4,128)(2,1)}, u32[]{:S(2)}, u32[]{:S(2)}) collective-permute-start(bf16[3,128]{1,0:T(4,128)(2,1)} %slice.150), channel_id=1, source_target_pairs={{0,4},{4,8},{8,12},{12,16},{16,20},{20,24},{24,28},{1,5},{5,9},{9,... | collective-permute-start | bytes 2312 | tf_op jit(solution)/shard_map/ppermute | solution.py:18
  191.5 10.1 %collective-permute-start.1 = (bf16[2,256]{1,0:T(2,128)(2,1)S(1)}, bf16[2,256]{1,0:T(2,128)(2,1)S(1)}, u32[]{:S(2)}, u32[]{:S(2)}) collective-permute-start(bf16[2,256]{1,0:T(2,128)(2,1)S(1)} %slice.131), channel_id=1, source_target_pairs={{0,4},{4,8},{8,12},{12,16},{16,20},{20,24},{24,28},{1,5},{5,9},{9,... | collective-permute-start | bytes 3080 | tf_op jit(solution)/shard_map/ppermute | solution.py:18
  193.0 8.6 %collective-permute-start = (bf16[2,256]{1,0:T(2,128)(2,1)}, bf16[2,256]{1,0:T(2,128)(2,1)S(1)}, u32[]{:S(2)}, u32[]{:S(2)}) collective-permute-start(bf16[2,256]{1,0:T(2,128)(2,1)} %slice.130), channel_id=1, source_target_pairs={{0,4},{4,8},{8,12},{12,16},{16,20},{20,24},{24,28},{1,5},{5,9},{9,... | collective-permute-start | bytes 3080 | tf_op jit(solution)/shard_map/ppermute | solution.py:18
  198.9 52.0 %copy-start.2 = (f32[512,128]{1,0:T(8,128)}, f32[512,128]{1,0:T(8,128)S(1)}, u32[]{:S(2)}) copy-start(f32[512,128]{1,0:T(8,128)S(1)} %divide_multiply_fusion.1) | copy-start | bytes 786436
  306.6 10.3 %copy-start.15 = (f32[4]{0:T(128)S(1)}, f32[4]{0:T(128)}, u32[]{:S(2)}) copy-start(f32[4]{0:T(128)} %param.42) | copy-start | bytes 52
  314.4 2.5 copy-start.3
  325.0 3.5 copy-start.12
  (3 other events, 5.6 us)
Sparse Core Ops, SparseCore 0:
  10.9 25.2 all-gather.10
  38.3 43.1 all-gather.20
  83.6 38.8 all-gather.14
  124.5 38.9 all-gather.16
  165.5 39.0 all-gather.12
  206.5 38.0 all-gather.18
  246.8 41.4 all-gather.22
  290.3 38.0 all-gather.24
  333.2 30.1 reduce-scatter.1
where the time goes:
time: 371 us; the launch traced here: 370 us
  waiting for transfers between devices  130 us (35%)
  blocking collectives  122 us (33%)
  matrix products  37.7 us (10%)
  other arithmetic  37.6 us (10%)
  local copies, waits for them, and re-layouts  14.8 us (4%)
  between operations  14.3 us (4%)
  starting transfers between devices  13 us (4%)
    all_gather x1, waiting for transfers between devices, per_device(): lax.all_gather(conv_output_weight, 'sp', axis=1, tiled=True)  40 us
    all_gather x1, waiting for transfers between devices, per_device(): lax.all_gather(value_weight_matrix, 'sp', axis=0, tiled=True)  35.7 us
    all_gather x1, blocking collectives, per_device(): lax.all_gather(write_key_weight, 'sp', axis=0, tiled=True)  35.2 us
    all_gather x1, blocking collectives, prefix(): lax.all_gather(part.astype(kind), axis)  33.8 us
    all_gather x1, blocking collectives, per_device(): lax.all_gather(read_key_weight, 'sp', axis=0, tiled=True)  33.7 us
    reduce_scatter x1, waiting for transfers between devices, per_device(): lax.psum_scatter((jnp.dot(mixer_part, wide_mixer, preferred_element_type=...  30.3 us
    unnamed x1, blocking collectives  19.2 us
    all_gather x1, waiting for transfers between devices, per_device(): lax.all_gather(inner_gate_weight, 'sp', axis=0, tiled=True)  13.8 us
  transfers between devices with their start and end apart: 14, of which 6 were waited for; matrix products, arithmetic and copies ran while one was open for 22% of the time, Pallas kernels for 0%

commit v1 on v0

--- a/solution.py
+++ b/solution.py
@@ -1,15 +1,544 @@
+import functools
+
 import jax
 import jax.numpy as jnp
 from jax import lax
+from jax.experimental import pallas as pl
+from jax.experimental.pallas import tpu as pltpu
 from jax.sharding import PartitionSpec as P
 
 HEAD_DIM = 64
 STATE = 128
-BLOCK = 64
-
-
+PLAIN_BLOCK = 64
+CHUNK = 128
+HALO = 16
+QIN = 2
+CORES = 2
 epsilon = 1e-05
 highest = lax.Precision.HIGHEST
+f32 = jnp.float32
+bf16 = jnp.bfloat16
+MESH = pl.DeviceIdType.MESH
+
+
+def nt(a, b, precision=None):
+    return lax.dot_general(
+        a, b, (((1,), (1,)), ((), ())), preferred_element_type=f32, precision=precision
+    )
+
+
+def silu(v):
+    return v / (1.0 + jnp.exp(-v))
+
+
+def kernel(
+    n,
+    T,
+    tokens,
+    in_scale,
+    w_outer,
+    w_inner,
+    w_value,
+    w_ogate,
+    w_state,
+    w_write,
+    w_read,
+    step_w,
+    taps_conv,
+    taps_in,
+    taps_wr,
+    taps_rd,
+    bias,
+    rate,
+    spikes,
+    direct,
+    hscale,
+    o_conv,
+    o_state,
+    out,
+    wbuf,
+    obuf,
+    norm,
+    acc,
+    mixbuf,
+    xbuf,
+    wrbuf,
+    rdbuf,
+    ybuf,
+    cumbuf,
+    stbuf,
+    st_send,
+    st_recv,
+    apart,
+    part,
+    r1,
+    p2,
+    r2,
+    loc_sem,
+    ws_sem,
+    wr_sem,
+    os_sem,
+    or_sem,
+    ts_sem,
+    tr_sem,
+    h_sem,
+    ss_sem,
+    sr_sem,
+    r1s_sem,
+    r1r_sem,
+    r2s_sem,
+    r2r_sem,
+):
+    sp = lax.axis_index("sp")
+    tp = lax.axis_index("tp")
+    rows, width = tokens.shape
+    kdim = w_outer.shape[0]
+    cdim = w_outer.shape[1]
+    half = wbuf.shape[3]
+    length = rows * T
+    heads_width = xbuf.shape[1]
+    heads = heads_width // HEAD_DIM
+    n_half = n // 2
+
+    barrier = pltpu.get_barrier_semaphore()
+    for d in range(1, n):
+        pl.semaphore_signal(
+            barrier, inc=1, device_id={"sp": lax.rem(sp + d, n)}, device_id_type=MESH
+        )
+    for d in range(1, T):
+        pl.semaphore_signal(
+            barrier, inc=1, device_id={"tp": lax.rem(tp + d, T)}, device_id_type=MESH
+        )
+
+    locals_ = []
+    at = 0
+    for ref in (w_outer, w_inner, w_value):
+        locals_.append((ref, wbuf.at[0, 0, :, at : at + ref.shape[1]]))
+        at += ref.shape[1]
+    at = 0
+    for ref in (w_ogate, w_state, w_write, w_read):
+        locals_.append((ref, wbuf.at[0, 1, :, at : at + ref.shape[1]]))
+        at += ref.shape[1]
+    locals_.append((o_conv, obuf.at[0, 0]))
+    locals_.append((o_state, obuf.at[0, 1]))
+    local_copies = [
+        pltpu.make_async_copy(src, dst, loc_sem.at[i]) for i, (src, dst) in enumerate(locals_)
+    ]
+    for copy in local_copies:
+        copy.start()
+
+    def pos_of(index):
+        odd = lax.rem(index, 2)
+        low = lax.div(index, 2)
+        return (1 - odd) * low + odd * (n - 1 - low)
+
+    def index_of(pos):
+        high = lax.div(pos, n_half)
+        return (1 - high) * 2 * pos + high * (2 * (n - 1 - pos) + 1)
+
+    pos = pos_of(sp)
+    right = index_of(lax.rem(pos + 1, n))
+    left = index_of(lax.rem(pos + n - 1, n))
+    neighbour = (right, left)
+
+    def owner_of(s, way):
+        return index_of(lax.rem(pos + n - s, n) if way == 0 else lax.rem(pos + s, n))
+
+    piece = kdim // QIN
+
+    def w_copy(s, q, way):
+        return pltpu.make_async_remote_copy(
+            src_ref=wbuf.at[s, way, pl.ds(q * piece, piece)],
+            dst_ref=wbuf.at[s + 1, way, pl.ds(q * piece, piece)],
+            send_sem=ws_sem.at[s, q, way],
+            recv_sem=wr_sem.at[s, q, way],
+            device_id={"sp": neighbour[way]},
+            device_id_type=MESH,
+        )
+
+    def o_copy(s, way):
+        return pltpu.make_async_remote_copy(
+            src_ref=obuf.at[s, way],
+            dst_ref=obuf.at[s + 1, way],
+            send_sem=os_sem.at[s, way],
+            recv_sem=or_sem.at[s, way],
+            device_id={"sp": neighbour[way]},
+            device_id_type=MESH,
+        )
+
+    def forward(s):
+        for q in range(QIN):
+            for way in range(2):
+
+                @pl.when(s > 0)
+                def _():
+                    w_copy(s - 1, q, way).wait_recv()
+
+                @pl.when(s < n - 1)
+                def _():
+                    w_copy(s, q, way).start()
+
+    def o_forward(s):
+        for way in range(2):
+
+            @pl.when(s > 0)
+            def _():
+                o_copy(s - 1, way).wait_recv()
+
+            @pl.when(s < n - 1)
+            def _():
+                o_copy(s, way).start()
+
+    own_at = pl.multiple_of(HALO + tp * rows, HALO)
+    x = tokens[...].astype(f32)
+    x = x * lax.rsqrt(jnp.mean(x * x, axis=1, keepdims=True) + epsilon)
+    norm[pl.ds(own_at, rows), :] = (x * in_scale[...].astype(f32)).astype(bf16)
+    acc[...] = jnp.zeros_like(acc)
+
+    for copy in local_copies:
+        copy.wait()
+    pl.semaphore_wait(barrier, n - 1 + T - 1)
+
+    forward(0)
+
+    def t_copy(d):
+        return pltpu.make_async_remote_copy(
+            src_ref=norm.at[pl.ds(own_at, rows)],
+            dst_ref=norm.at[pl.ds(own_at, rows)],
+            send_sem=ts_sem.at[d],
+            recv_sem=tr_sem.at[d],
+            device_id={"tp": lax.rem(tp + d, T)},
+            device_id_type=MESH,
+        )
+
+    for d in range(1, T):
+        t_copy(d).start()
+
+    mid = n_half - 1
+
+    def ahead(s, carry):
+        forward(s)
+        return carry
+
+    lax.fori_loop(1, max(mid, 1), ahead, 0)
+
+    def t_wait(d):
+        source = pl.multiple_of(HALO + lax.rem(tp + T - d, T) * rows, HALO)
+        pltpu.make_async_remote_copy(
+            src_ref=norm.at[pl.ds(source, rows)],
+            dst_ref=norm.at[pl.ds(source, rows)],
+            send_sem=ts_sem.at[d],
+            recv_sem=tr_sem.at[d],
+            device_id={"tp": lax.rem(tp + d, T)},
+            device_id_type=MESH,
+        ).wait_recv()
+
+    for d in range(1, T):
+        t_wait(d)
+
+    def h_copy():
+        return pltpu.make_async_remote_copy(
+            src_ref=norm.at[pl.ds(length, HALO)],
+            dst_ref=norm.at[pl.ds(0, HALO)],
+            send_sem=h_sem.at[0],
+            recv_sem=h_sem.at[1],
+            device_id={"sp": lax.rem(sp + 1, n)},
+            device_id_type=MESH,
+        )
+
+    @pl.when(sp < n - 1)
+    def _():
+        h_copy().start()
+
+    forward(max(mid, 1))
+
+    @pl.when(sp > 0)
+    def _():
+        h_copy().wait_recv()
+
+    @pl.when(sp == 0)
+    def _():
+        norm[0:HALO, :] = jnp.zeros((HALO, width), bf16)
+
+    def project(s):
+        for way in range(2):
+            at = pl.multiple_of(owner_of(s, way) * kdim, kdim)
+            lhs = norm[:, pl.ds(at, kdim)]
+            for c in range(0, half, 256):
+                acc[:, way * half + c : way * half + c + 256] += jnp.dot(
+                    lhs, wbuf[s, way, :, c : c + 256], preferred_element_type=f32
+                )
+
+    start = max(mid, 1)
+
+    def body(s, carry):
+        @pl.when(s > start)
+        def _():
+            forward(s)
+
+        project(s)
+
+        @pl.when(s - start < start)
+        def _():
+            project(s - start)
+
+        return carry
+
+    lax.fori_loop(start, n, body, 0)
+
+    o_forward(0)
+    o_done = [1]
+    stages = 2 * (length // CHUNK)
+    per_stage = -(-(n - 1) // max(stages - 1, 1))
+
+    def relay(k=per_stage):
+        lo = o_done[0]
+        hi = min(lo + k, n)
+        o_done[0] = hi
+        for s in range(lo, hi) if hi - lo <= 4 else ():
+            o_forward(s)
+        if hi - lo > 4:
+
+            def go(s, carry):
+                o_forward(s)
+                return carry
+
+            lax.fori_loop(lo, hi, go, 0)
+
+    step = jax.nn.softplus(nt(step_w[...], norm[HALO:, :])[0:8] + bias[...])
+    logs = -step * jnp.exp(rate[...]) + spikes[...]
+    r_id = lax.broadcasted_iota(jnp.int32, (CHUNK, CHUNK), 0)
+    c_id = lax.broadcasted_iota(jnp.int32, (CHUNK, CHUNK), 1)
+    causal = r_id >= c_id
+    lower = causal.astype(f32)
+    eye = (r_id == c_id).astype(f32)
+    lane = lax.broadcasted_iota(jnp.int32, (1, heads_width), 1)
+
+    def spread(columns):
+        full = jnp.broadcast_to(columns[:, 0:1], (columns.shape[0], heads_width))
+        for h in range(1, heads):
+            full = jnp.where(lane >= h * HEAD_DIM, columns[:, h : h + 1], full)
+        return full
+
+    def taps(u, weights):
+        k_taps = weights.shape[0]
+        w = weights[...].astype(f32)
+        total = w[k_taps - 1 : k_taps] * u[8:]
+        for k in range(k_taps - 1):
+            total = total + w[k : k + 1] * pltpu.roll(u, k_taps - 1 - k, 0)[8:]
+        return total
+
+    blocks = length // CHUNK
+    running = jnp.zeros((STATE, heads_width), f32)
+    before = jnp.zeros((1, heads_width), f32)
+    at_outer, at_inner, at_value, at_ogate, at_state = (i * cdim for i in range(5))
+    at_write = 5 * cdim
+    at_read = at_write + STATE
+    for b in range(blocks):
+        t0 = b * CHUNK
+        take = slice(t0 + HALO - 8, t0 + HALO + CHUNK)
+        own = slice(t0 + HALO, t0 + HALO + CHUNK)
+
+        def field(begin, size, span):
+            return acc[span, begin : begin + size].astype(bf16).astype(f32)
+
+        product = field(at_inner, cdim, take) * field(at_value, cdim, take)
+        mix = field(at_outer, cdim, own) * taps(product, taps_conv)
+        apart[t0 : t0 + CHUNK, 0:cdim] = mix.astype(bf16)
+        xs = silu(taps(field(at_state, cdim, take), taps_in))
+        wr = silu(taps(field(at_write, STATE, take), taps_wr))
+        rd = silu(taps(field(at_read, STATE, take), taps_rd))
+        span = slice(t0, t0 + CHUNK)
+        cum = nt(lower, logs[:, span], highest)
+        steps = nt(eye, step[:, span], highest)
+        cum_wide = spread(cum)
+        weighted = xs * spread(steps)
+        xbuf[span, :] = xs
+        mixbuf[span, :] = weighted.astype(bf16)
+        wrbuf[span, :] = wr.astype(bf16)
+        rdbuf[span, :] = rd.astype(bf16)
+        cumbuf[span, :] = cum_wide
+        last = cum_wide[CHUNK - 1 : CHUNK]
+        scaled = (weighted * jnp.exp(last - cum_wide)).astype(bf16)
+        stbuf[b] = running
+        running = running * jnp.exp(last) + jnp.dot(
+            wr.T.astype(bf16), scaled, preferred_element_type=f32
+        )
+        before = before + last
+        relay()
+    st_send[0:STATE, :] = running.astype(bf16)
+    st_send[STATE:, :] = jnp.broadcast_to(jnp.exp(before), (HALO, heads_width)).astype(bf16)
+
+    def s_copy(k, slot):
+        return pltpu.make_async_remote_copy(
+            src_ref=st_send,
+            dst_ref=st_recv.at[slot],
+            send_sem=ss_sem.at[k],
+            recv_sem=sr_sem.at[slot],
+            device_id={"sp": k},
+            device_id_type=MESH,
+        )
+
+    def within(b):
+        t0 = b * CHUNK
+        span = slice(t0, t0 + CHUNK)
+        scores = nt(rdbuf[span, :], wrbuf[span, :])
+        cum_t = lax.dot_general(
+            logs[:, span], lower, (((1,), (1,)), ((), ())),
+            preferred_element_type=f32, precision=highest,
+        )
+        for pair in range(0, heads_width, 128):
+            both = []
+            for h in range(pair // HEAD_DIM, (pair + 128) // HEAD_DIM):
+                diff = cumbuf[span, h * HEAD_DIM : h * HEAD_DIM + 1] - cum_t[h : h + 1, :]
+                damped = scores * jnp.exp(jnp.where(causal, diff, -1e30))
+                both.append(
+                    jnp.dot(
+                        damped.astype(bf16), mixbuf[span, pair : pair + 128],
+                        preferred_element_type=f32,
+                    )
+                )
+            first = lax.broadcasted_iota(jnp.int32, (1, 128), 1) < HEAD_DIM
+            ybuf[span, pair : pair + 128] = jnp.where(first, both[0], both[1])
+
+    def s_start(k, carry):
+        s_copy(k, sp).start()
+        return carry
+
+    lax.fori_loop(sp + 1, n, s_start, 0)
+    for b in range(blocks):
+        within(b)
+        relay()
+    relay(n)
+
+    def s_take(k, arriving):
+        s_copy(k, k).wait_recv()
+        got = st_recv[k].astype(f32)
+        return arriving * got[STATE : STATE + 1] + got[0:STATE]
+
+    arriving = lax.fori_loop(0, sp, s_take, jnp.zeros((STATE, heads_width), f32))
+
+    group = (
+        lax.div(lax.broadcasted_iota(jnp.int32, (heads_width, heads_width), 0), HEAD_DIM)
+        == lax.div(lax.broadcasted_iota(jnp.int32, (heads_width, heads_width), 1), HEAD_DIM)
+    ).astype(bf16)
+    before = jnp.zeros((1, heads_width), f32)
+    for b in range(blocks):
+        t0 = b * CHUNK
+        span = slice(t0, t0 + CHUNK)
+        own = slice(t0 + HALO, t0 + HALO + CHUNK)
+        cum_wide = cumbuf[span, :]
+        entering = (stbuf[b] + jnp.exp(before) * arriving).astype(bf16)
+        before = before + cum_wide[CHUNK - 1 : CHUNK]
+        head_out = (
+            ybuf[span, :]
+            + jnp.dot(rdbuf[span, :], entering, preferred_element_type=f32) * jnp.exp(cum_wide)
+            + direct[...] * xbuf[span, :]
+        )
+        og = acc[own, at_ogate : at_ogate + cdim].astype(bf16).astype(f32)
+        gated = head_out * silu(og)
+        square = jnp.dot((gated * gated).astype(bf16), group, preferred_element_type=f32)
+        normalized = gated * lax.rsqrt(square * (1.0 / HEAD_DIM) + epsilon)
+        apart[span, cdim:] = (normalized * hscale[...].astype(f32)).astype(bf16)
+
+    ocols = o_conv.shape[1]
+
+    def project_out(k, carry):
+        kp = pos_of(k)
+        a = lax.rem(pos + n - kp, n)
+        c = lax.rem(kp + n - pos, n)
+        cols = pl.ds(pl.multiple_of(k * ocols, ocols), ocols)
+        part[:, cols] = (
+            jnp.dot(apart[:, 0:cdim], obuf[a, 0], preferred_element_type=f32)
+            + jnp.dot(apart[:, cdim:], obuf[c, 1], preferred_element_type=f32)
+        ).astype(bf16)
+        return carry
+
+    Y = T // CORES
+    core = lax.rem(tp, CORES)
+    chip = lax.div(tp, CORES)
+    partner = chip * CORES + 1 - core
+    pieces = r1.shape[1]
+    pcols = width // pieces
+
+    def block_rows(y, c):
+        return pl.ds(pl.multiple_of((y * CORES + c) * rows, rows), rows)
+
+    def r1_copy(d, c):
+        y = lax.rem(chip + d, Y)
+        return pltpu.make_async_remote_copy(
+            src_ref=part.at[block_rows(y, 1 - core), pl.ds(c * pcols, pcols)],
+            dst_ref=r1.at[d, c],
+            send_sem=r1s_sem.at[d, c],
+            recv_sem=r1r_sem.at[d, c],
+            device_id={"tp": partner},
+            device_id_type=MESH,
+        )
+
+    def r2_copy(d, c):
+        return pltpu.make_async_remote_copy(
+            src_ref=p2.at[d, c],
+            dst_ref=r2.at[d, c],
+            send_sem=r2s_sem.at[d, c],
+            recv_sem=r2r_sem.at[d, c],
+            device_id={"tp": lax.rem(chip + d, Y) * CORES + core},
+            device_id_type=MESH,
+        )
+
+    per_piece = n // pieces
+    for c in range(pieces):
+        lax.fori_loop(c * per_piece, (c + 1) * per_piece, project_out, 0)
+        for d in range(1, Y):
+            r1_copy(d, c).start()
+        r1_copy(0, c).start()
+        if c > 0:
+            for d in range(1, Y):
+                reduce_far(d, c - 1, r1_copy, r2_copy, part, r1, p2, block_rows, chip, Y, core, pcols)
+    for d in range(1, Y):
+        reduce_far(d, pieces - 1, r1_copy, r2_copy, part, r1, p2, block_rows, chip, Y, core, pcols)
+    for c in range(pieces):
+        r1_copy(0, c).wait_recv()
+        cols = slice(c * pcols, (c + 1) * pcols)
+        total = part[block_rows(chip, core), cols].astype(f32) + r1[0, c].astype(f32)
+        for d in range(1, Y):
+            r2_copy(d, c).wait_recv()
+            total = total + r2[d, c].astype(f32)
+        out[:, cols] = total.astype(bf16)
+
+    def w_drain(s, carry):
+        for way in range(2):
+            for q in range(QIN):
+                w_copy(s, q, way).wait_send()
+            o_copy(s, way).wait_send()
+        return carry
+
+    lax.fori_loop(0, n - 1, w_drain, 0)
+    for d in range(1, T):
+        t_copy(d).wait_send()
+
+    @pl.when(sp < n - 1)
+    def _():
+        h_copy().wait_send()
+
+    def s_drain(k, carry):
+        s_copy(k, sp).wait_send()
+        return carry
+
+    lax.fori_loop(sp + 1, n, s_drain, 0)
+    for c in range(pieces):
+        for d in range(Y):
+            r1_copy(d, c).wait_send()
+        for d in range(1, Y):
+            r2_copy(d, c).wait_send()
+
+
+def reduce_far(d, c, r1_copy, r2_copy, part, r1, p2, block_rows, chip, Y, core, pcols):
+    r1_copy(d, c).wait_recv()
+    y = lax.rem(chip + d, Y)
+    p2[d, c] = (
+        part[block_rows(y, core), c * pcols : (c + 1) * pcols].astype(f32) + r1[d, c].astype(f32)
+    ).astype(bf16)
+    r2_copy(d, c).start()
 
 
 def shifted(shard, axis, by):
@@ -55,7 +584,7 @@
     return (earlier[0] * later[0], earlier[1] * later[0][:, None, None] + later[1])
 
 
-def per_device(
+def plain_path(
     tokens,
     input_norm_scale,
     outer_gate_weight,
@@ -146,16 +675,16 @@
     heads_here = discrete_step.shape[1]
     groups_here = seq_write.shape[1] // STATE
     per_group = heads_here // groups_here
-    blocks = length // BLOCK
-    input_blocks = seq_input.reshape(blocks, BLOCK, heads_here, HEAD_DIM)
-    weighted = input_blocks * discrete_step.reshape(blocks, BLOCK, heads_here, 1)
+    blocks = length // PLAIN_BLOCK
+    input_blocks = seq_input.reshape(blocks, PLAIN_BLOCK, heads_here, HEAD_DIM)
+    weighted = input_blocks * discrete_step.reshape(blocks, PLAIN_BLOCK, heads_here, 1)
     write_blocks = jnp.repeat(
-        seq_write.reshape(blocks, BLOCK, groups_here, STATE), per_group, axis=2
-    )
-    read_blocks = jnp.repeat(seq_read.reshape(blocks, BLOCK, groups_here, STATE), per_group, axis=2)
-    cumulative = jnp.cumsum(step_logarithm.reshape(blocks, BLOCK, heads_here), axis=1)
-    causal = lax.broadcasted_iota(jnp.int32, (BLOCK, BLOCK), 0) >= lax.broadcasted_iota(
-        jnp.int32, (BLOCK, BLOCK), 1
+        seq_write.reshape(blocks, PLAIN_BLOCK, groups_here, STATE), per_group, axis=2
+    )
+    read_blocks = jnp.repeat(seq_read.reshape(blocks, PLAIN_BLOCK, groups_here, STATE), per_group, axis=2)
+    cumulative = jnp.cumsum(step_logarithm.reshape(blocks, PLAIN_BLOCK, heads_here), axis=1)
+    causal = lax.broadcasted_iota(jnp.int32, (PLAIN_BLOCK, PLAIN_BLOCK), 0) >= lax.broadcasted_iota(
+        jnp.int32, (PLAIN_BLOCK, PLAIN_BLOCK), 1
     )
     scores = jnp.einsum("clhm,cshm->clsh", read_blocks, write_blocks, precision=highest)
     damping = jnp.exp(
@@ -218,29 +747,97 @@
     )
 
 
+def per_device(
+    tokens, input_norm_scale, outer_gate_weight, inner_gate_weight, value_weight_matrix,
+    output_gate_weight, state_input_weight, write_key_weight, read_key_weight, step_size_weight,
+    gated_conv_weight, input_conv_weight, write_conv_weight, read_conv_weight, step_size_bias,
+    log_decay_rate, decay_spikes, direct_path_weight, head_norm_scale, conv_output_weight,
+    state_output_weight,
+):
+    n, T = lax.axis_size("sp"), lax.axis_size("tp")
+    rows, width = tokens.shape
+    kdim, cdim = outer_gate_weight.shape
+    heads = step_size_bias.shape[0]
+    hw = heads * HEAD_DIM
+    half = 3 * cdim
+    length = rows * T
+    ocols = conv_output_weight.shape[1]
+    if kdim % 128 or ocols % 128 or n % 2 or T % CORES or write_key_weight.shape[1] != STATE:
+        return plain_path(
+            tokens, input_norm_scale, outer_gate_weight, inner_gate_weight,
+            value_weight_matrix, output_gate_weight, state_input_weight, write_key_weight,
+            read_key_weight, step_size_weight, gated_conv_weight, input_conv_weight,
+            write_conv_weight, read_conv_weight, step_size_bias, log_decay_rate, decay_spikes,
+            direct_path_weight, head_norm_scale, conv_output_weight, state_output_weight,
+        )
+    Y = T // CORES
+    pieces = 4 if n % 4 == 0 else 1
+    pad = 8 - heads
+    step_w = jnp.pad(step_size_weight.T, ((0, 16 - heads), (0, 0)))
+    bias = jnp.pad(step_size_bias, (0, pad))[:, None]
+    rate = jnp.pad(log_decay_rate, (0, pad))[:, None]
+    spikes = jnp.pad(decay_spikes, ((0, pad), (0, 0)))
+    direct = jnp.repeat(direct_path_weight, HEAD_DIM)[None, :]
+    vm = pl.BlockSpec(memory_space=pltpu.VMEM)
+    hbm = pl.BlockSpec(memory_space=pl.ANY)
+    dma = pltpu.SemaphoreType.DMA
+    return pl.pallas_call(
+        functools.partial(kernel, n, T),
+        out_shape=jax.ShapeDtypeStruct((rows, width), bf16),
+        in_specs=[vm] * 2 + [hbm] * 7 + [vm] * 10 + [hbm] * 2,
+        out_specs=vm,
+        scratch_shapes=[
+            pltpu.VMEM((n, 2, kdim, half), bf16),
+            pltpu.VMEM((n, 2, cdim, ocols), bf16),
+            pltpu.VMEM((HALO + length, width), bf16),
+            pltpu.VMEM((HALO + length, 2 * half), f32),
+            pltpu.VMEM((length, hw), bf16),
+            pltpu.VMEM((length, hw), f32),
+            pltpu.VMEM((length, STATE), bf16),
+            pltpu.VMEM((length, STATE), bf16),
+            pltpu.VMEM((length, hw), f32),
+            pltpu.VMEM((length, hw), f32),
+            pltpu.VMEM((length // CHUNK, STATE, hw), f32),
+            pltpu.VMEM((STATE + HALO, hw), bf16),
+            pltpu.VMEM((n, STATE + HALO, hw), bf16),
+            pltpu.VMEM((length, cdim + hw), bf16),
+            pltpu.VMEM((length, width), bf16),
+            pltpu.VMEM((Y, pieces, rows, width // pieces), bf16),
+            pltpu.VMEM((Y, pieces, rows, width // pieces), bf16),
+            pltpu.VMEM((Y, pieces, rows, width // pieces), bf16),
+            dma((9,)),
+            dma((n, QIN, 2)),
+            dma((n, QIN, 2)),
+            dma((n, 2)),
+            dma((n, 2)),
+            dma((T,)),
+            dma((T,)),
+            dma((2,)),
+            dma((n,)),
+            dma((n,)),
+            dma((Y, pieces)),
+            dma((Y, pieces)),
+            dma((Y, pieces)),
+            dma((Y, pieces)),
+        ],
+        compiler_params=pltpu.CompilerParams(
+            collective_id=0, has_side_effects=True, vmem_limit_bytes=62 * 1024 * 1024
+        ),
+    )(
+        tokens, input_norm_scale[None, :], outer_gate_weight, inner_gate_weight,
+        value_weight_matrix, output_gate_weight, state_input_weight, write_key_weight,
+        read_key_weight, step_w, gated_conv_weight, input_conv_weight, write_conv_weight,
+        read_conv_weight, bias, rate, spikes, direct, head_norm_scale[None, :],
+        conv_output_weight, state_output_weight,
+    )
+
+
 def solution(mesh):
     placed = (
-        P(("sp", "tp"), None),
-        P(),
-        P("sp", "tp"),
-        P("sp", "tp"),
-        P("sp", "tp"),
-        P("sp", "tp"),
-        P("sp", "tp"),
-        P("sp", "tp"),
-        P("sp", "tp"),
-        P(None, "tp"),
-        P(None, "tp"),
-        P(None, "tp"),
-        P(None, "tp"),
-        P(None, "tp"),
-        P("tp"),
-        P("tp"),
-        P("tp", "sp"),
-        P("tp"),
-        P("tp"),
-        P("tp", "sp"),
-        P("tp", "sp"),
+        (P(("sp", "tp"), None), P())
+        + (P("sp", "tp"),) * 7
+        + (P(None, "tp"),) * 5
+        + (P("tp"), P("tp"), P("tp", "sp"), P("tp"), P("tp"), P("tp", "sp"), P("tp", "sp"))
     )
     return jax.shard_map(
         per_device, mesh=mesh, in_specs=placed, out_specs=P(("sp", "tp"), None), check_vma=False

time: 371 us -> 136 us (0.37)
  waiting for transfers between devices: 130 us -> 0 us
  Pallas kernels: 0 us -> 126 us
  blocking collectives: 122 us -> 0 us
  matrix products: 37.7 us -> 0 us
  other arithmetic: 37.6 us -> 0 us
  between operations: 14.3 us -> 0.02 us
  starting transfers between devices: 13 us -> 0 us
  local copies, waits for them, and re-layouts: 14.8 us -> 8.35 us
    pallas_call x0 -> x1, Pallas kernels: none -> 126 us  [per_device(): pl.pallas_call(functools.partial(kernel, n, T), out_shape=jax.ShapeDtypeS...]
    all_gather x3 -> x0, blocking collectives: 103 us -> none  [the longest x1 35.2 us: per_device(): lax.all_gather(write_key_weight, 'sp', axis=0, tiled=True)]
    all_gather x8 -> x0, waiting for transfers between devices: 95.5 us -> none  [the longest x1 40 us: per_device(): lax.all_gather(conv_output_weight, 'sp', axis=1, tiled=True)]
    dot_general x13 -> x0, matrix products: 37.7 us -> none  [the longest x6 13.1 us: per_device(): jnp.dot(normed, weight_rows, preferred_element_type=jnp.float32)]
    reduce_scatter x1 -> x0, waiting for transfers between devices: 30.3 us -> none  [per_device(): lax.psum_scatter((jnp.dot(mixer_part, wide_mixer, preferred_element_type=...]
    unnamed x1 -> x0, blocking collectives: 19.2 us -> none
    ppermute x5 -> x0, starting transfers between devices: 12.7 us -> none  [shifted(): return lax.ppermute(shard, axis, pairs)]
    add x8 -> x0, other arithmetic: 7.93 us -> none  [advance(): carried_state * jnp.exp(block_log)[:, None, None] + contribution]
  transfers between devices with their start and end apart: 14 -> 0, of which waited for: 6 -> 0; matrix products, arithmetic and copies ran while one was open for 22% -> 0% of each run, Pallas kernels for 0% -> 0%
where the time goes in v1:
time: 136 us; the launch traced here: 134 us
  Pallas kernels  126 us (93%)
  local copies, waits for them, and re-layouts  8.35 us (6%)
    pallas_call x1, Pallas kernels, per_device(): pl.pallas_call(functools.partial(kernel, n, T), out_shape=jax.ShapeDtypeS...  126 us
    unnamed x15, local copies, waits for them, and re-layouts  3.96 us

profile of v1, /device:TPU:0, one launch (start us, length us, event | category | flops | bytes accessed | tf_op | source)
XLA Modules:
  0.0 133.9 jit_solution(15380613442207778677)
XLA Ops:
  0.0 0.0 copy-start.4
  0.0 0.7 copy-done.4
  0.7 0.0 copy-start.5
  0.7 0.6 copy-done.5
  1.3 0.0 copy-start.6
  1.3 0.6 copy-done.6
  2.0 0.0 copy-start.3
  2.0 0.5 broadcast_in_dim.19.hscale
  2.5 0.1 copy-done.3
  2.6 0.1 broadcast_in_dim.18
  2.7 0.6 broadcast_in_dim_reshape.3.direct
  3.3 0.0 copy-start.2
  3.3 0.7 copy.23.rate
  4.0 0.0 copy-start.1
  4.0 0.7 copy.22.bias
  4.7 0.0 copy-done.2
  4.7 0.0 copy-start
  4.7 0.6 broadcast_in_dim.15.in_scale
  5.2 0.0 copy-done.1
  5.2 0.6 pad.18.spikes
  5.8 0.0 copy-done
  5.8 0.6 pad.15.step_w
  6.5 125.5 %shard_map.199 = bf16[128,2048]{1,0:T(8,128)(2,1)} custom-call(bf16[128,2048]{1,0:T(8,128)(2,1)} %tokens.1, bf16[1,2048]{1,0:T(2,128)(2,1)} %broadcast_in_dim.15.in_scale, bf16[256,256]{1,0:T(8,128)(2,1)} %w_outer.1, bf16[256,256]{1,0:T(8,128)(2,1)} %w_inner.1, bf16[256,256]{1,0:T(8,128)(2,1)} %w_value.1, bf16[256,256]{1,0:T(8,128)(2,1)} %w_ogate.1, ...), custom_call_target="tpu_custom_call" | custom-call | tf_op jit(solution)/shard_map/pallas_call | solution.py:784
  132.0 1.9 %copy.25 = bf16[128,2048]{1,0:T(8,128)(2,1)} copy(bf16[128,2048]{1,0:T(8,128)(2,1)} %shard_map.199) | data formatting | bytes 1048576
  (2 shorter events, 0.0 us)
Async XLA Ops:
  0.0 0.7 copy-start.4
  0.7 0.7 copy-start.5
  1.3 0.7 copy-start.6
  2.0 0.7 copy-start.3
  3.3 1.3 copy-start.2
  4.0 1.3 copy-start.1
  4.7 1.2 copy-start

commit v2 on v1

--- a/solution.py
+++ b/solution.py
@@ -13,6 +13,7 @@
 CHUNK = 128
 HALO = 16
 QIN = 2
+QOUT = 2
 CORES = 2
 epsilon = 1e-05
 highest = lax.Precision.HIGHEST
@@ -69,6 +70,9 @@
     stbuf,
     st_send,
     st_recv,
+    e_send,
+    e_recv,
+    pair_buf,
     apart,
     part,
     r1,
@@ -82,8 +86,8 @@
     ts_sem,
     tr_sem,
     h_sem,
-    ss_sem,
-    sr_sem,
+    x_sem,
+    e_sem,
     r1s_sem,
     r1r_sem,
     r2s_sem,
@@ -119,8 +123,11 @@
     for ref in (w_ogate, w_state, w_write, w_read):
         locals_.append((ref, wbuf.at[0, 1, :, at : at + ref.shape[1]]))
         at += ref.shape[1]
-    locals_.append((o_conv, obuf.at[0, 0]))
-    locals_.append((o_state, obuf.at[0, 1]))
+    ohalf = obuf.shape[3]
+    for way in range(2):
+        cut = pl.ds(way * ohalf, ohalf)
+        locals_.append((o_conv.at[:, cut], obuf.at[0, way, pl.ds(0, cdim)]))
+        locals_.append((o_state.at[:, cut], obuf.at[0, way, pl.ds(cdim, heads_width)]))
     local_copies = [
         pltpu.make_async_copy(src, dst, loc_sem.at[i]) for i, (src, dst) in enumerate(locals_)
     ]
@@ -156,12 +163,14 @@
             device_id_type=MESH,
         )
 
-    def o_copy(s, way):
+    opiece = obuf.shape[2] // QOUT
+
+    def o_copy(s, q, way):
         return pltpu.make_async_remote_copy(
-            src_ref=obuf.at[s, way],
-            dst_ref=obuf.at[s + 1, way],
-            send_sem=os_sem.at[s, way],
-            recv_sem=or_sem.at[s, way],
+            src_ref=obuf.at[s, way, pl.ds(q * opiece, opiece)],
+            dst_ref=obuf.at[s + 1, way, pl.ds(q * opiece, opiece)],
+            send_sem=os_sem.at[s, q, way],
+            recv_sem=or_sem.at[s, q, way],
             device_id={"sp": neighbour[way]},
             device_id_type=MESH,
         )
@@ -179,15 +188,16 @@
                     w_copy(s, q, way).start()
 
     def o_forward(s):
-        for way in range(2):
-
-            @pl.when(s > 0)
-            def _():
-                o_copy(s - 1, way).wait_recv()
-
-            @pl.when(s < n - 1)
-            def _():
-                o_copy(s, way).start()
+        for q in range(QOUT):
+            for way in range(2):
+
+                @pl.when(s > 0)
+                def _():
+                    o_copy(s - 1, q, way).wait_recv()
+
+                @pl.when(s < n - 1)
+                def _():
+                    o_copy(s, q, way).start()
 
     own_at = pl.multiple_of(HALO + tp * rows, HALO)
     x = tokens[...].astype(f32)
@@ -276,6 +286,10 @@
         def _():
             forward(s)
 
+        @pl.when(s == max(n - 2, start))
+        def _():
+            o_forward(0)
+
         project(s)
 
         @pl.when(s - start < start)
@@ -286,27 +300,15 @@
 
     lax.fori_loop(start, n, body, 0)
 
-    o_forward(0)
-    o_done = [1]
-    stages = 2 * (length // CHUNK)
-    per_stage = -(-(n - 1) // max(stages - 1, 1))
-
-    def relay(k=per_stage):
-        lo = o_done[0]
-        hi = min(lo + k, n)
-        o_done[0] = hi
-        for s in range(lo, hi) if hi - lo <= 4 else ():
-            o_forward(s)
-        if hi - lo > 4:
-
-            def go(s, carry):
-                o_forward(s)
-                return carry
-
-            lax.fori_loop(lo, hi, go, 0)
-
-    step = jax.nn.softplus(nt(step_w[...], norm[HALO:, :])[0:8] + bias[...])
-    logs = -step * jnp.exp(rate[...]) + spikes[...]
+    def column(ref):
+        index = lax.broadcasted_iota(jnp.int32, (heads, 1), 0)
+        full = jnp.full((heads, 1), ref[0], f32)
+        for h in range(1, heads):
+            full = jnp.where(index == h, ref[h], full)
+        return full
+
+    step = jax.nn.softplus(nt(step_w[...], norm[HALO:, :])[0:heads] + column(bias))
+    logs = -step * jnp.exp(column(rate)) + spikes[...]
     r_id = lax.broadcasted_iota(jnp.int32, (CHUNK, CHUNK), 0)
     c_id = lax.broadcasted_iota(jnp.int32, (CHUNK, CHUNK), 1)
     causal = r_id >= c_id
@@ -365,19 +367,35 @@
             wr.T.astype(bf16), scaled, preferred_element_type=f32
         )
         before = before + last
-        relay()
     st_send[0:STATE, :] = running.astype(bf16)
     st_send[STATE:, :] = jnp.broadcast_to(jnp.exp(before), (HALO, heads_width)).astype(bf16)
 
-    def s_copy(k, slot):
+    z = lax.div(sp, 2)
+    second = lax.rem(sp, 2)
+    depth = n_half
+
+    def x_copy():
         return pltpu.make_async_remote_copy(
             src_ref=st_send,
-            dst_ref=st_recv.at[slot],
-            send_sem=ss_sem.at[k],
-            recv_sem=sr_sem.at[slot],
-            device_id={"sp": k},
+            dst_ref=st_recv,
+            send_sem=x_sem.at[0],
+            recv_sem=x_sem.at[1],
+            device_id={"sp": sp + 1 - 2 * second},
             device_id_type=MESH,
         )
+
+    def e_copy():
+        return pltpu.make_async_remote_copy(
+            src_ref=e_send,
+            dst_ref=e_recv,
+            send_sem=e_sem.at[0],
+            recv_sem=e_sem.at[1],
+            device_id={"sp": lax.rem(sp + 2, n)},
+            device_id_type=MESH,
+        )
+
+    x_copy().start()
+    o_next = 1
 
     def within(b):
         t0 = b * CHUNK
@@ -401,115 +419,157 @@
             first = lax.broadcasted_iota(jnp.int32, (1, 128), 1) < HEAD_DIM
             ybuf[span, pair : pair + 128] = jnp.where(first, both[0], both[1])
 
-    def s_start(k, carry):
-        s_copy(k, sp).start()
-        return carry
-
-    lax.fori_loop(sp + 1, n, s_start, 0)
     for b in range(blocks):
+        if b % 2 == 0 and o_next < n:
+            o_forward(o_next)
+            o_next += 1
         within(b)
-        relay()
-    relay(n)
-
-    def s_take(k, arriving):
-        s_copy(k, k).wait_recv()
-        got = st_recv[k].astype(f32)
-        return arriving * got[STATE : STATE + 1] + got[0:STATE]
-
-    arriving = lax.fori_loop(0, sp, s_take, jnp.zeros((STATE, heads_width), f32))
+    x_copy().wait_recv()
+    other = st_recv[0:STATE, :].astype(f32)
+    other_decay = st_recv[STATE : STATE + 1, :].astype(f32)
+    own_decay = jnp.exp(before)
+    is_second = jnp.broadcast_to(second, (1, heads_width)) == 1
+    pair_buf[0] = jnp.where(
+        is_second, other * own_decay + running, running * other_decay + other
+    )
+    pair_buf[1] = jnp.where(is_second, other, jnp.zeros_like(other))
+    pair_decay = own_decay * other_decay
+    first_decay = jnp.where(is_second, other_decay, jnp.ones_like(other_decay))
 
     group = (
         lax.div(lax.broadcasted_iota(jnp.int32, (heads_width, heads_width), 0), HEAD_DIM)
         == lax.div(lax.broadcasted_iota(jnp.int32, (heads_width, heads_width), 1), HEAD_DIM)
     ).astype(bf16)
-    before = jnp.zeros((1, heads_width), f32)
-    for b in range(blocks):
-        t0 = b * CHUNK
-        span = slice(t0, t0 + CHUNK)
-        own = slice(t0 + HALO, t0 + HALO + CHUNK)
-        cum_wide = cumbuf[span, :]
-        entering = (stbuf[b] + jnp.exp(before) * arriving).astype(bf16)
-        before = before + cum_wide[CHUNK - 1 : CHUNK]
-        head_out = (
-            ybuf[span, :]
-            + jnp.dot(rdbuf[span, :], entering, preferred_element_type=f32) * jnp.exp(cum_wide)
-            + direct[...] * xbuf[span, :]
-        )
-        og = acc[own, at_ogate : at_ogate + cdim].astype(bf16).astype(f32)
-        gated = head_out * silu(og)
-        square = jnp.dot((gated * gated).astype(bf16), group, preferred_element_type=f32)
-        normalized = gated * lax.rsqrt(square * (1.0 / HEAD_DIM) + epsilon)
-        apart[span, cdim:] = (normalized * hscale[...].astype(f32)).astype(bf16)
-
-    ocols = o_conv.shape[1]
-
-    def project_out(k, carry):
-        kp = pos_of(k)
-        a = lax.rem(pos + n - kp, n)
-        c = lax.rem(kp + n - pos, n)
-        cols = pl.ds(pl.multiple_of(k * ocols, ocols), ocols)
-        part[:, cols] = (
-            jnp.dot(apart[:, 0:cdim], obuf[a, 0], preferred_element_type=f32)
-            + jnp.dot(apart[:, cdim:], obuf[c, 1], preferred_element_type=f32)
-        ).astype(bf16)
+    direct_wide = jnp.full((1, heads_width), direct[0], f32)
+    for h in range(1, heads):
+        direct_wide = jnp.where(lane >= h * HEAD_DIM, direct[h], direct_wide)
+
+    def finish():
+        before = jnp.zeros((1, heads_width), f32)
+        arriving = pair_buf[1] + first_decay * pair_buf[2]
+        for b in range(blocks):
+            t0 = b * CHUNK
+            span = slice(t0, t0 + CHUNK)
+            own = slice(t0 + HALO, t0 + HALO + CHUNK)
+            cum_wide = cumbuf[span, :]
+            entering = (stbuf[b] + jnp.exp(before) * arriving).astype(bf16)
+            before = before + cum_wide[CHUNK - 1 : CHUNK]
+            head_out = (
+                ybuf[span, :]
+                + jnp.dot(rdbuf[span, :], entering, preferred_element_type=f32) * jnp.exp(cum_wide)
+                + direct_wide * xbuf[span, :]
+            )
+            og = acc[own, at_ogate : at_ogate + cdim].astype(bf16).astype(f32)
+            gated = head_out * silu(og)
+            square = jnp.dot((gated * gated).astype(bf16), group, preferred_element_type=f32)
+            normalized = gated * lax.rsqrt(square * (1.0 / HEAD_DIM) + epsilon)
+            apart[span, cdim:] = (normalized * hscale[...].astype(f32)).astype(bf16)
+
+    def link(j, carry):
+        @pl.when(z == j)
+        def _():
+            @pl.when(j == 0)
+            def _():
+                pair_buf[2] = jnp.zeros_like(pair_buf[2])
+
+            @pl.when(j > 0)
+            def _():
+                e_copy().wait_recv()
+                pair_buf[2] = e_recv[...].astype(f32)
+
+            @pl.when(j < depth - 1)
+            def _():
+                e_send[...] = (pair_buf[2] * pair_decay + pair_buf[0]).astype(bf16)
+                e_copy().start()
+
+            finish()
+
+        @pl.when(o_next + j < n)
+        def _():
+            o_forward(o_next + j)
+
         return carry
+
+    lax.fori_loop(0, depth, link, 0)
+    o_next = min(o_next + depth, n)
 
     Y = T // CORES
     core = lax.rem(tp, CORES)
     chip = lax.div(tp, CORES)
     partner = chip * CORES + 1 - core
-    pieces = r1.shape[1]
-    pcols = width // pieces
+    ocols = 2 * ohalf
 
     def block_rows(y, c):
         return pl.ds(pl.multiple_of((y * CORES + c) * rows, rows), rows)
 
-    def r1_copy(d, c):
-        y = lax.rem(chip + d, Y)
+    def r1_copy(d, s):
         return pltpu.make_async_remote_copy(
-            src_ref=part.at[block_rows(y, 1 - core), pl.ds(c * pcols, pcols)],
-            dst_ref=r1.at[d, c],
-            send_sem=r1s_sem.at[d, c],
-            recv_sem=r1r_sem.at[d, c],
+            src_ref=part.at[s, block_rows(lax.rem(chip + d, Y), 1 - core)],
+            dst_ref=r1.at[d, s],
+            send_sem=r1s_sem.at[d, s],
+            recv_sem=r1r_sem.at[d, s],
             device_id={"tp": partner},
             device_id_type=MESH,
         )
 
-    def r2_copy(d, c):
+    def r2_copy(d, s):
         return pltpu.make_async_remote_copy(
-            src_ref=p2.at[d, c],
-            dst_ref=r2.at[d, c],
-            send_sem=r2s_sem.at[d, c],
-            recv_sem=r2r_sem.at[d, c],
+            src_ref=p2.at[d, s],
+            dst_ref=r2.at[d, s],
+            send_sem=r2s_sem.at[d, s],
+            recv_sem=r2r_sem.at[d, s],
             device_id={"tp": lax.rem(chip + d, Y) * CORES + core},
             device_id_type=MESH,
         )
 
-    per_piece = n // pieces
-    for c in range(pieces):
-        lax.fori_loop(c * per_piece, (c + 1) * per_piece, project_out, 0)
+    def reduce_far(s):
         for d in range(1, Y):
-            r1_copy(d, c).start()
-        r1_copy(0, c).start()
-        if c > 0:
-            for d in range(1, Y):
-                reduce_far(d, c - 1, r1_copy, r2_copy, part, r1, p2, block_rows, chip, Y, core, pcols)
-    for d in range(1, Y):
-        reduce_far(d, pieces - 1, r1_copy, r2_copy, part, r1, p2, block_rows, chip, Y, core, pcols)
-    for c in range(pieces):
-        r1_copy(0, c).wait_recv()
-        cols = slice(c * pcols, (c + 1) * pcols)
-        total = part[block_rows(chip, core), cols].astype(f32) + r1[0, c].astype(f32)
+            r1_copy(d, s).wait_recv()
+            mine = part[s, block_rows(lax.rem(chip + d, Y), core), :]
+            p2[d, s] = (mine.astype(f32) + r1[d, s].astype(f32)).astype(bf16)
+            r2_copy(d, s).start()
+
+    def project_out(s, carry):
+        @pl.when(s >= o_next)
+        def _():
+            o_forward(s)
+
+        for way in range(2):
+            part[s, :, way * ohalf : (way + 1) * ohalf] = jnp.dot(
+                apart[...], obuf[s, way], preferred_element_type=f32
+            ).astype(bf16)
         for d in range(1, Y):
-            r2_copy(d, c).wait_recv()
-            total = total + r2[d, c].astype(f32)
-        out[:, cols] = total.astype(bf16)
+            r1_copy(d, s).start()
+        r1_copy(0, s).start()
+
+        @pl.when(s > 0)
+        def _():
+            reduce_far(s - 1)
+
+        return carry
+
+    lax.fori_loop(0, n, project_out, 0)
+    reduce_far(n - 1)
+
+    def collect(s, carry):
+        r1_copy(0, s).wait_recv()
+        total = part[s, block_rows(chip, core), :].astype(f32) + r1[0, s].astype(f32)
+        for d in range(1, Y):
+            r2_copy(d, s).wait_recv()
+            total = total + r2[d, s].astype(f32)
+        for way in range(2):
+            at = pl.multiple_of(owner_of(s, way) * ocols + way * ohalf, ohalf)
+            out[:, pl.ds(at, ohalf)] = total[:, way * ohalf : (way + 1) * ohalf].astype(bf16)
+        return carry
+
+    lax.fori_loop(0, n, collect, 0)
 
     def w_drain(s, carry):
         for way in range(2):
             for q in range(QIN):
                 w_copy(s, q, way).wait_send()
-            o_copy(s, way).wait_send()
+            for q in range(QOUT):
+                o_copy(s, q, way).wait_send()
         return carry
 
     lax.fori_loop(0, n - 1, w_drain, 0)
@@ -520,25 +580,20 @@
     def _():
         h_copy().wait_send()
 
-    def s_drain(k, carry):
-        s_copy(k, sp).wait_send()
+    x_copy().wait_send()
+
+    @pl.when(z < depth - 1)
+    def _():
+        e_copy().wait_send()
+
+    def r_drain(s, carry):
+        for d in range(Y):
+            r1_copy(d, s).wait_send()
+        for d in range(1, Y):
+            r2_copy(d, s).wait_send()
         return carry
 
-    lax.fori_loop(sp + 1, n, s_drain, 0)
-    for c in range(pieces):
-        for d in range(Y):
-            r1_copy(d, c).wait_send()
-        for d in range(1, Y):
-            r2_copy(d, c).wait_send()
-
-
-def reduce_far(d, c, r1_copy, r2_copy, part, r1, p2, block_rows, chip, Y, core, pcols):
-    r1_copy(d, c).wait_recv()
-    y = lax.rem(chip + d, Y)
-    p2[d, c] = (
-        part[block_rows(y, core), c * pcols : (c + 1) * pcols].astype(f32) + r1[d, c].astype(f32)
-    ).astype(bf16)
-    r2_copy(d, c).start()
+    lax.fori_loop(0, n, r_drain, 0)
 
 
 def shifted(shard, axis, by):
@@ -762,7 +817,7 @@
     half = 3 * cdim
     length = rows * T
     ocols = conv_output_weight.shape[1]
-    if kdim % 128 or ocols % 128 or n % 2 or T % CORES or write_key_weight.shape[1] != STATE:
+    if kdim % 128 or ocols % 256 or n % 2 or T % CORES or write_key_weight.shape[1] != STATE:
         return plain_path(
             tokens, input_norm_scale, outer_gate_weight, inner_gate_weight,
             value_weight_matrix, output_gate_weight, state_input_weight, write_key_weight,
@@ -771,24 +826,19 @@
             direct_path_weight, head_norm_scale, conv_output_weight, state_output_weight,
         )
     Y = T // CORES
-    pieces = 4 if n % 4 == 0 else 1
-    pad = 8 - heads
     step_w = jnp.pad(step_size_weight.T, ((0, 16 - heads), (0, 0)))
-    bias = jnp.pad(step_size_bias, (0, pad))[:, None]
-    rate = jnp.pad(log_decay_rate, (0, pad))[:, None]
-    spikes = jnp.pad(decay_spikes, ((0, pad), (0, 0)))
-    direct = jnp.repeat(direct_path_weight, HEAD_DIM)[None, :]
     vm = pl.BlockSpec(memory_space=pltpu.VMEM)
+    sm = pl.BlockSpec(memory_space=pltpu.SMEM)
     hbm = pl.BlockSpec(memory_space=pl.ANY)
     dma = pltpu.SemaphoreType.DMA
     return pl.pallas_call(
         functools.partial(kernel, n, T),
         out_shape=jax.ShapeDtypeStruct((rows, width), bf16),
-        in_specs=[vm] * 2 + [hbm] * 7 + [vm] * 10 + [hbm] * 2,
+        in_specs=[vm] * 2 + [hbm] * 7 + [vm] * 5 + [sm] * 2 + [vm, sm, vm] + [hbm] * 2,
         out_specs=vm,
         scratch_shapes=[
             pltpu.VMEM((n, 2, kdim, half), bf16),
-            pltpu.VMEM((n, 2, cdim, ocols), bf16),
+            pltpu.VMEM((n, 2, cdim + hw, ocols // 2), bf16),
             pltpu.VMEM((HALO + length, width), bf16),
             pltpu.VMEM((HALO + length, 2 * half), f32),
             pltpu.VMEM((length, hw), bf16),
@@ -799,26 +849,29 @@
             pltpu.VMEM((length, hw), f32),
             pltpu.VMEM((length // CHUNK, STATE, hw), f32),
             pltpu.VMEM((STATE + HALO, hw), bf16),
-            pltpu.VMEM((n, STATE + HALO, hw), bf16),
+            pltpu.VMEM((STATE + HALO, hw), bf16),
+            pltpu.VMEM((STATE, hw), bf16),
+            pltpu.VMEM((STATE, hw), bf16),
+            pltpu.VMEM((3, STATE, hw), f32),
             pltpu.VMEM((length, cdim + hw), bf16),
-            pltpu.VMEM((length, width), bf16),
-            pltpu.VMEM((Y, pieces, rows, width // pieces), bf16),
-            pltpu.VMEM((Y, pieces, rows, width // pieces), bf16),
-            pltpu.VMEM((Y, pieces, rows, width // pieces), bf16),
-            dma((9,)),
+            pltpu.VMEM((n, length, ocols), bf16),
+            pltpu.VMEM((Y, n, rows, ocols), bf16),
+            pltpu.VMEM((Y, n, rows, ocols), bf16),
+            pltpu.VMEM((Y, n, rows, ocols), bf16),
+            dma((11,)),
             dma((n, QIN, 2)),
             dma((n, QIN, 2)),
-            dma((n, 2)),
-            dma((n, 2)),
+            dma((n, QOUT, 2)),
+            dma((n, QOUT, 2)),
             dma((T,)),
             dma((T,)),
             dma((2,)),
-            dma((n,)),
-            dma((n,)),
-            dma((Y, pieces)),
-            dma((Y, pieces)),
-            dma((Y, pieces)),
-            dma((Y, pieces)),
+            dma((2,)),
+            dma((2,)),
+            dma((Y, n)),
+            dma((Y, n)),
+            dma((Y, n)),
+            dma((Y, n)),
         ],
         compiler_params=pltpu.CompilerParams(
             collective_id=0, has_side_effects=True, vmem_limit_bytes=62 * 1024 * 1024
@@ -827,7 +880,8 @@
         tokens, input_norm_scale[None, :], outer_gate_weight, inner_gate_weight,
         value_weight_matrix, output_gate_weight, state_input_weight, write_key_weight,
         read_key_weight, step_w, gated_conv_weight, input_conv_weight, write_conv_weight,
-        read_conv_weight, bias, rate, spikes, direct, head_norm_scale[None, :],
+        read_conv_weight, step_size_bias, log_decay_rate, decay_spikes, direct_path_weight,
+        head_norm_scale[None, :],
         conv_output_weight, state_output_weight,
     )
 

time: 136 us -> 118 us (0.87); the launches traced: 134 us -> 118 us
  Pallas kernels: 126 us -> 112 us
  local copies, waits for them, and re-layouts: 8.35 us -> 5.76 us
    pallas_call x1, Pallas kernels: 126 us -> 112 us  [per_device(): pl.pallas_call(functools.partial(kernel, n, T), out_shape=jax.ShapeDtypeS...]
    unnamed x15 -> x3, local copies, waits for them, and re-layouts: 3.96 us -> 2.54 us
    broadcast_in_dim x5 -> x0, local copies, waits for them, and re-layouts: 1.41 us -> none  [the longest x2 0.68 us: per_device(): bias = jnp.pad(step_size_bias, (0, pad))[:, None]]
where the time goes in v2:
time: 118 us
  Pallas kernels  112 us (95%)
  local copies, waits for them, and re-layouts  5.76 us (5%)
    pallas_call x1, Pallas kernels, per_device(): pl.pallas_call(functools.partial(kernel, n, T), out_shape=jax.ShapeDtypeS...  112 us
    unnamed x3, local copies, waits for them, and re-layouts  2.54 us

profile of v2, /device:TPU:0, one launch (start us, length us, event | category | flops | bytes accessed | tf_op | source)
XLA Modules:
  0.0 118.1 jit_solution(2136901714448374878)
XLA Ops:
  0.0 0.0 copy-start
  0.0 0.7 copy-done
  0.7 0.6 broadcast_in_dim.7.hscale
  1.2 1.3 %broadcast_in_dim.6.in_scale = bf16[1,2048]{1,0:T(2,128)(2,1)} reshape(bf16[2048]{0:T(1024)(128)(2,1)} %param.22) | data formatting | bytes 8192 | tf_op jit(solution)/shard_map/broadcast_in_dim | solution.py:880
  2.5 1.4 %pad.4.step_w = bf16[16,2048]{1,0:T(8,128)(2,1)} pad(bf16[4,2048]{1,0:T(4,128)(2,1)} %bitcast.1, bf16[]{:T(256)} %constant.2.clone.1), padding=0_12x0_0 | pad | bytes 81922 | tf_op jit(solution)/shard_map/jit(_pad)/pad | solution.py:829
  3.9 112.4 %shard_map.199 = bf16[128,2048]{1,0:T(8,128)(2,1)} custom-call(bf16[128,2048]{1,0:T(8,128)(2,1)} %tokens.1, bf16[1,2048]{1,0:T(2,128)(2,1)} %broadcast_in_dim.6.in_scale, bf16[256,256]{1,0:T(8,128)(2,1)} %w_outer.1, bf16[256,256]{1,0:T(8,128)(2,1)} %w_inner.1, bf16[256,256]{1,0:T(8,128)(2,1)} %w_value.1, bf16[256,256]{1,0:T(8,128)(2,1)} %w_ogate.1, ...), custom_call_target="tpu_custom_call" | custom-call | tf_op jit(solution)/shard_map/pallas_call | solution.py:834
  116.3 1.9 %copy.23 = bf16[128,2048]{1,0:T(8,128)(2,1)} copy(bf16[128,2048]{1,0:T(8,128)(2,1)} %shard_map.199) | data formatting | bytes 1048576
Async XLA Ops:
  0.0 0.7 copy-start

commit v3 on v2

--- a/solution.py
+++ b/solution.py
@@ -202,7 +202,7 @@
     own_at = pl.multiple_of(HALO + tp * rows, HALO)
     x = tokens[...].astype(f32)
     x = x * lax.rsqrt(jnp.mean(x * x, axis=1, keepdims=True) + epsilon)
-    norm[pl.ds(own_at, rows), :] = (x * in_scale[...].astype(f32)).astype(bf16)
+    norm[pl.ds(own_at, rows), :] = (x * in_scale[...].astype(f32).reshape(1, width)).astype(bf16)
     acc[...] = jnp.zeros_like(acc)
 
     for copy in local_copies:
@@ -307,7 +307,7 @@
             full = jnp.where(index == h, ref[h], full)
         return full
 
-    step = jax.nn.softplus(nt(step_w[...], norm[HALO:, :])[0:heads] + column(bias))
+    step = jax.nn.softplus(jnp.dot(norm[HALO:, :], step_w[...], preferred_element_type=f32).T + column(bias))
     logs = -step * jnp.exp(column(rate)) + spikes[...]
     r_id = lax.broadcasted_iota(jnp.int32, (CHUNK, CHUNK), 0)
     c_id = lax.broadcasted_iota(jnp.int32, (CHUNK, CHUNK), 1)
@@ -463,35 +463,7 @@
             gated = head_out * silu(og)
             square = jnp.dot((gated * gated).astype(bf16), group, preferred_element_type=f32)
             normalized = gated * lax.rsqrt(square * (1.0 / HEAD_DIM) + epsilon)
-            apart[span, cdim:] = (normalized * hscale[...].astype(f32)).astype(bf16)
-
-    def link(j, carry):
-        @pl.when(z == j)
-        def _():
-            @pl.when(j == 0)
-            def _():
-                pair_buf[2] = jnp.zeros_like(pair_buf[2])
-
-            @pl.when(j > 0)
-            def _():
-                e_copy().wait_recv()
-                pair_buf[2] = e_recv[...].astype(f32)
-
-            @pl.when(j < depth - 1)
-            def _():
-                e_send[...] = (pair_buf[2] * pair_decay + pair_buf[0]).astype(bf16)
-                e_copy().start()
-
-            finish()
-
-        @pl.when(o_next + j < n)
-        def _():
-            o_forward(o_next + j)
-
-        return carry
-
-    lax.fori_loop(0, depth, link, 0)
-    o_next = min(o_next + depth, n)
+            apart[span, cdim:] = (normalized * hscale[...].astype(f32).reshape(1, heads_width)).astype(bf16)
 
     Y = T // CORES
     core = lax.rem(tp, CORES)
@@ -530,10 +502,6 @@
             r2_copy(d, s).start()
 
     def project_out(s, carry):
-        @pl.when(s >= o_next)
-        def _():
-            o_forward(s)
-
         for way in range(2):
             part[s, :, way * ohalf : (way + 1) * ohalf] = jnp.dot(
                 apart[...], obuf[s, way], preferred_element_type=f32
@@ -548,7 +516,44 @@
 
         return carry
 
-    lax.fori_loop(0, n, project_out, 0)
+    def link(j, carry):
+        @pl.when(z == j)
+        def _():
+            @pl.when(j == 0)
+            def _():
+                pair_buf[2] = jnp.zeros_like(pair_buf[2])
+
+            @pl.when(j > 0)
+            def _():
+                e_copy().wait_recv()
+                pair_buf[2] = e_recv[...].astype(f32)
+
+            @pl.when(j < depth - 1)
+            def _():
+                e_send[...] = (pair_buf[2] * pair_decay + pair_buf[0]).astype(bf16)
+                e_copy().start()
+
+            finish()
+            lax.fori_loop(0, o_next + j, project_out, 0)
+
+        @pl.when(o_next + j < n)
+        def _():
+            o_forward(o_next + j)
+
+            @pl.when(z <= j)
+            def _():
+                project_out(o_next + j, 0)
+
+        return carry
+
+    lax.fori_loop(0, depth, link, 0)
+
+    def rest(s, carry):
+        o_forward(s)
+        project_out(s, 0)
+        return carry
+
+    lax.fori_loop(min(o_next + depth, n), n, rest, 0)
     reduce_far(n - 1)
 
     def collect(s, carry):
@@ -826,7 +831,6 @@
             direct_path_weight, head_norm_scale, conv_output_weight, state_output_weight,
         )
     Y = T // CORES
-    step_w = jnp.pad(step_size_weight.T, ((0, 16 - heads), (0, 0)))
     vm = pl.BlockSpec(memory_space=pltpu.VMEM)
     sm = pl.BlockSpec(memory_space=pltpu.SMEM)
     hbm = pl.BlockSpec(memory_space=pl.ANY)
@@ -877,11 +881,11 @@
             collective_id=0, has_side_effects=True, vmem_limit_bytes=62 * 1024 * 1024
         ),
     )(
-        tokens, input_norm_scale[None, :], outer_gate_weight, inner_gate_weight,
+        tokens, input_norm_scale, outer_gate_weight, inner_gate_weight,
         value_weight_matrix, output_gate_weight, state_input_weight, write_key_weight,
-        read_key_weight, step_w, gated_conv_weight, input_conv_weight, write_conv_weight,
+        read_key_weight, step_size_weight, gated_conv_weight, input_conv_weight, write_conv_weight,
         read_conv_weight, step_size_bias, log_decay_rate, decay_spikes, direct_path_weight,
-        head_norm_scale[None, :],
+        head_norm_scale,
         conv_output_weight, state_output_weight,
     )
 

time: 118 us -> 113 us (0.958)
  Pallas kernels: 112 us -> 109 us
  local copies, waits for them, and re-layouts: 5.76 us -> 3.65 us
    pallas_call x1, Pallas kernels: 112 us -> 109 us  [per_device(): pl.pallas_call(functools.partial(kernel, n, T), out_shape=jax.ShapeDtypeS...]
    broadcast_in_dim x2 -> x0, local copies, waits for them, and re-layouts: 1.87 us -> none  [the longest x1 1.28 us: per_device(): input_norm_scale[None, :]]
    pad x1 -> x0, local copies, waits for them, and re-layouts: 1.36 us -> none  [per_device(): step_w = jnp.pad(step_size_weight.T, ((0, 16 - heads), (0, 0)))]
    unnamed x3 -> x2, local copies, waits for them, and re-layouts: 2.54 us -> 3.65 us
where the time goes in v3:
time: 113 us
  Pallas kernels  109 us (96%)
  local copies, waits for them, and re-layouts  3.65 us (3%)
    pallas_call x1, Pallas kernels, per_device(): pl.pallas_call(functools.partial(kernel, n, T), out_shape=jax.ShapeDtypeS...  109 us
    unnamed x2, local copies, waits for them, and re-layouts  3.65 us

profile of v3, /device:TPU:0, one launch (start us, length us, event | category | flops | bytes accessed | tf_op | source)
XLA Modules:
  0.0 112.6 jit_solution(14108800712061375082)
XLA Ops:
  0.0 1.8 %copy.22.step_w = bf16[2048,4]{1,0:T(8,128)(2,1)} copy(bf16[2048,4]{0,1:T(4,128)(2,1)} %param.30) | data formatting | bytes 32768 | tf_op args[9]
  1.8 109.0 %shard_map.199 = bf16[128,2048]{1,0:T(8,128)(2,1)} custom-call(bf16[128,2048]{1,0:T(8,128)(2,1)} %tokens.1, bf16[2048]{0:T(1024)(128)(2,1)} %in_scale.1, bf16[256,256]{1,0:T(8,128)(2,1)} %w_outer.1, bf16[256,256]{1,0:T(8,128)(2,1)} %w_inner.1, bf16[256,256]{1,0:T(8,128)(2,1)} %w_value.1, bf16[256,256]{1,0:T(8,128)(2,1)} %w_ogate.1, ...), custom_call_target="tpu_custom_call" | custom-call | tf_op jit(solution)/shard_map/pallas_call | solution.py:838
  110.7 1.9 %copy.24 = bf16[128,2048]{1,0:T(8,128)(2,1)} copy(bf16[128,2048]{1,0:T(8,128)(2,1)} %shard_map.199) | data formatting | bytes 1048576

commit v4 on v3

--- a/solution.py
+++ b/solution.py
@@ -534,15 +534,18 @@
                 e_copy().start()
 
             finish()
-            lax.fori_loop(0, o_next + j, project_out, 0)
 
         @pl.when(o_next + j < n)
         def _():
             o_forward(o_next + j)
 
-            @pl.when(z <= j)
+            @pl.when(z < j)
             def _():
                 project_out(o_next + j, 0)
+
+            @pl.when(z == j)
+            def _():
+                lax.fori_loop(0, o_next + j + 1, project_out, 0)
 
         return carry
 
@@ -822,7 +825,7 @@
     half = 3 * cdim
     length = rows * T
     ocols = conv_output_weight.shape[1]
-    if kdim % 128 or ocols % 256 or n % 2 or T % CORES or write_key_weight.shape[1] != STATE:
+    if kdim % 128 or ocols % 256 or n % 2 or n < 6 or T % CORES or write_key_weight.shape[1] != STATE:
         return plain_path(
             tokens, input_norm_scale, outer_gate_weight, inner_gate_weight,
             value_weight_matrix, output_gate_weight, state_input_weight, write_key_weight,

time: 113 us -> 113 us (level)
  no operation moved by 1% of the time
where the time goes in v4:
time: 113 us; the launch traced here: 112 us
  Pallas kernels  109 us (96%)
  local copies, waits for them, and re-layouts  3.65 us (3%)
    pallas_call x1, Pallas kernels, per_device(): pl.pallas_call(functools.partial(kernel, n, T), out_shape=jax.ShapeDtypeS...  109 us
    unnamed x2, local copies, waits for them, and re-layouts  3.65 us

profile of v4, /device:TPU:0, one launch (start us, length us, event | category | flops | bytes accessed | tf_op | source)
XLA Modules:
  0.0 112.3 jit_solution(5674530052460726714)
XLA Ops:
  0.0 1.8 %copy.22.step_w = bf16[2048,4]{1,0:T(8,128)(2,1)} copy(bf16[2048,4]{0,1:T(4,128)(2,1)} %param.30) | data formatting | bytes 32768 | tf_op args[9]
  1.8 108.6 %shard_map.199 = bf16[128,2048]{1,0:T(8,128)(2,1)} custom-call(bf16[128,2048]{1,0:T(8,128)(2,1)} %tokens.1, bf16[2048]{0:T(1024)(128)(2,1)} %in_scale.1, bf16[256,256]{1,0:T(8,128)(2,1)} %w_outer.1, bf16[256,256]{1,0:T(8,128)(2,1)} %w_inner.1, bf16[256,256]{1,0:T(8,128)(2,1)} %w_value.1, bf16[256,256]{1,0:T(8,128)(2,1)} %w_ogate.1, ...), custom_call_target="tpu_custom_call" | custom-call | tf_op jit(solution)/shard_map/pallas_call | solution.py:841
  110.4 1.9 %copy.24 = bf16[128,2048]{1,0:T(8,128)(2,1)} copy(bf16[128,2048]{1,0:T(8,128)(2,1)} %shard_map.199) | data formatting | bytes 1048576
